TPU v7x, 256 devices: a whole 4x4x8 slice. The times are simulated.
256 devices in a mesh: sp: 64 (over z, y, core), tp: 4 (over x).
Axes of the slice: x: 4, y: 4, z: 8, core: 2. Of those that a mesh axis runs over, the one named last changes fastest.
Arguments:
- queries: bfloat16 [16384, 2048], P('sp', 'tp'), may hold values from -9 to 9
- keys: bfloat16 [16384, 1024], P('sp', 'tp'), may hold values from -9 to 9
- values: bfloat16 [16384, 1024], P('sp', 'tp'), may hold values from -6 to 6
- lam: float32 [8], P('tp'), may hold values from 0.3 to 0.8
- diff_gain: float32 [256], replicated, may hold values from 0.1 to 1.9
- lin_query: bfloat16 [16384, 512], P('sp', 'tp'), may hold values from -6 to 6
- lin_key: bfloat16 [16384, 512], P('sp', 'tp'), may hold values from -6 to 6
- lin_value: bfloat16 [16384, 1024], P('sp', 'tp'), may hold values from -6 to 6
- decay_pre: float32 [16384, 512], P('sp', 'tp'), may hold values from -14 to 14
- lin_gain: float32 [1024], P('tp'), may hold values from 0.1 to 1.9
- w_out_diff: bfloat16 [2048, 4096], P('tp'), may hold values from -0.125 to 0.125
- w_out_lin: bfloat16 [1024, 4096], P('tp'), may hold values from -0.1875 to 0.1875
Outputs:
- mixed: bfloat16 [16384, 4096], P(('sp', 'tp'))
All inputs are finite; a program needn't handle non-finite values.
Results may differ from a plain program's by a relative error of at most 0.015.
Values may be sent and summed in bfloat16 or wider, within the bound.
A program may use at most 128 MiB of HBM per device.

v0:
```python
import math

import jax
import jax.numpy as jnp
from jax import lax
from jax.sharding import Mesh
from jax.sharding import PartitionSpec as P

HEAD_DIM = 128
KEY_DIM = 128
VAL_DIM = 256
BLOCK = 64
SP = ("sp_0", "sp_1", "sp_2")
SP_TP = ("sp_0", "sp_1", "sp_2", "tp")


norm_eps = 1e-06
gate_temp = 16.0
neg_large = -1e30


def side_by_side(arrays, axis, dim, along):
    widths = [a.shape[along] for a in arrays]
    both = jnp.concatenate(arrays, axis=along)
    out = lax.all_gather(both, axis, axis=dim, tiled=True)
    return tuple(jnp.split(out, [sum(widths[:k]) for k in range(1, len(widths))], axis=along))


def filled_with(array, identity):
    return jax.tree.map(
        lambda a, e: jnp.broadcast_to(jnp.asarray(e, a.dtype), a.shape), array, identity
    )


def entering(array, axes, combine, identity):
    before = start = filled_with(array, identity)
    subtotal = array
    for axis in reversed(axes):
        size, mine = (lax.axis_size(axis), lax.axis_index(axis))
        pieces = jax.tree.map(
            lambda part, kind: lax.all_gather(part.astype(kind), axis),
            subtotal,
            (jnp.bfloat16, jnp.bfloat16),
        )
        inside, subtotal = (start, start)
        for k in range(size):
            passed = k < mine
            subtotal = combine(
                subtotal, jax.tree.map(lambda part, own: part[k].astype(own.dtype), pieces, array)
            )
            inside = jax.tree.map(lambda new, old: jnp.where(passed, new, old), subtotal, inside)
        before = combine(inside, before)
    return before


def split_up(array, dim, size):
    dims = array.shape
    blocks = array.reshape(*dims[:dim], size, dims[dim] // size, *dims[dim + 1 :])
    return jnp.moveaxis(blocks, dim, 0)


def summed_on_arrival(array, axis, dim):
    blocks = split_up(array, dim, lax.axis_size(axis))
    arrived = lax.all_to_all(blocks, axis, split_axis=0, concat_axis=0, tiled=True)
    return arrived.astype(jnp.float32).sum(axis=0)


def head_norm(mixed_in, gain):
    return (
        mixed_in
        * lax.rsqrt(jnp.mean(mixed_in * mixed_in, axis=-1, keepdims=True) + norm_eps)
        * gain
    )


def span_rows(row_count):
    return math.gcd(row_count, 2048)


def attend(carries, query_maps, key_maps, value_rows, query_pos):
    row_count = value_rows.shape[0]
    step_rows = span_rows(row_count)
    last_query = query_pos[-1]

    def visit(step_index, current):
        first_row = step_index * step_rows
        key_pos = first_row + jnp.arange(step_rows, dtype=jnp.int32)

        def compute(kept):
            value_part = lax.dynamic_slice_in_dim(value_rows, first_row, step_rows, 0)
            allowed = query_pos[:, None] >= key_pos[None, :]
            updated = []
            for query_map, key_map, running in zip(query_maps, key_maps, kept):
                old_top, old_total, old_numer = running
                key_part = lax.dynamic_slice_in_dim(key_map, first_row, step_rows, 0)
                scores = jnp.einsum(
                    "gjqd,sgd->gjqs", query_map, key_part, preferred_element_type=jnp.float32
                ) / math.sqrt(HEAD_DIM)
                scores = jnp.where(allowed, scores, neg_large)
                new_top = jnp.maximum(old_top, jnp.max(scores, axis=-1))
                weights = jnp.where(allowed, jnp.exp(scores - new_top[..., None]), 0.0)
                shrink = jnp.exp(old_top - new_top)
                new_total = old_total * shrink + jnp.sum(weights, axis=-1)
                new_numer = old_numer * shrink[..., None] + jnp.einsum(
                    "gjqs,sge->gjqe",
                    weights.astype(jnp.bfloat16),
                    value_part,
                    preferred_element_type=jnp.float32,
                )
                updated.append((new_top, new_total, new_numer))
            return tuple(updated)

        return lax.cond(first_row <= last_query, compute, lambda kept: kept, current)

    return lax.fori_loop(0, row_count // step_rows, visit, carries)


def decay_block(carry, inputs):
    run_state, passed = carry
    query_blk, key_blk, value_blk, decay_blk = inputs
    length = query_blk.shape[1]
    cumulative = jnp.cumsum(decay_blk, axis=1)
    lower_mask = jnp.tril(jnp.ones((length, length), dtype=bool))[None, :, :, None]
    spread = jnp.where(lower_mask, cumulative[:, :, None, :] - cumulative[:, None, :, :], 0.0)
    factor = jnp.where(lower_mask, jnp.exp(spread), 0.0)
    inner = jnp.einsum("htd,hsd,htsd->hts", query_blk, key_blk, factor)
    local_part = jnp.einsum("hts,hse->hte", inner, value_blk)
    carried = jnp.einsum("htd,hde->hte", query_blk * jnp.exp(cumulative), run_state)
    last_sum = cumulative[:, -1:, :]
    new_state = jnp.exp(last_sum[:, 0, :])[..., None] * run_state + jnp.einsum(
        "hsd,hse->hde", key_blk * jnp.exp(last_sum - cumulative), value_blk
    )
    reach = query_blk * jnp.exp(passed[:, None, :] + cumulative)
    return ((new_state, passed + last_sum[:, 0, :]), (local_part + carried, reach))


def chain(earlier, later):
    return (earlier[0] + later[0], jnp.exp(later[0])[..., None] * earlier[1] + later[1])


def body(
    queries,
    keys,
    values,
    lam,
    diff_gain,
    lin_query,
    lin_key,
    lin_value,
    decay_pre,
    lin_gain,
    w_out_diff,
    w_out_lin,
):
    tok_rows = queries.shape[0]
    kv_here = keys.shape[1] // (2 * HEAD_DIM)
    heads_here = queries.shape[1] // (2 * HEAD_DIM)
    group_size = heads_here // kv_here
    query_pos = lax.axis_index(SP) * tok_rows + jnp.arange(tok_rows, dtype=jnp.int32)
    query_grid = queries.reshape(tok_rows, kv_here, group_size, 2, HEAD_DIM)
    query_maps = (
        query_grid[:, :, :, 0].transpose(1, 2, 0, 3),
        query_grid[:, :, :, 1].transpose(1, 2, 0, 3),
    )
    key_grid = keys.reshape(tok_rows, kv_here, 2, HEAD_DIM)
    value_grid = values.reshape(tok_rows, kv_here, VAL_DIM)
    blank = (
        jnp.full((kv_here, group_size, tok_rows), neg_large, jnp.float32),
        jnp.zeros((kv_here, group_size, tok_rows), jnp.float32),
        jnp.zeros((kv_here, group_size, tok_rows, VAL_DIM), jnp.float32),
    )
    pieces = side_by_side((key_grid[:, :, 0], value_grid), SP, 0, 2)
    (first_acc,) = attend((blank,), query_maps[:1], (pieces[0],), pieces[1], query_pos)
    pieces = side_by_side((key_grid[:, :, 1], value_grid), SP, 0, 2)
    (second_acc,) = attend((blank,), query_maps[1:], (pieces[0],), pieces[1], query_pos)
    lam_grid = lam.reshape(kv_here, group_size)
    attended = first_acc[2] / first_acc[1][..., None] - lam_grid[..., None, None] * (
        second_acc[2] / second_acc[1][..., None]
    )
    diff_out = head_norm(attended, diff_gain).astype(jnp.bfloat16)
    diff_out = diff_out.transpose(2, 0, 1, 3).reshape(tok_rows, heads_here * VAL_DIM)
    lin_heads_here = lin_query.shape[1] // KEY_DIM
    block_count = tok_rows // BLOCK

    def arrange(array, width):
        return (
            array.astype(jnp.float32)
            .reshape(block_count, BLOCK, lin_heads_here, width)
            .transpose(0, 2, 1, 3)
        )

    start_carry = (
        jnp.zeros((lin_heads_here, KEY_DIM, VAL_DIM), jnp.float32),
        jnp.zeros((lin_heads_here, KEY_DIM), jnp.float32),
    )
    (end_state, end_decay), (local_out, reach) = lax.scan(
        decay_block,
        start_carry,
        (
            arrange(lin_query, KEY_DIM) * KEY_DIM ** (-0.5),
            arrange(lin_key, KEY_DIM),
            arrange(lin_value, VAL_DIM),
            arrange(jax.nn.log_sigmoid(decay_pre) / gate_temp, KEY_DIM),
        ),
    )
    incoming = entering(
        (end_decay, end_state), SP, chain, (jnp.zeros_like(end_decay), jnp.zeros_like(end_state))
    )
    linear_rows = local_out + jnp.einsum("nhtd,hde->nhte", reach, incoming[1])
    linear_rows = linear_rows.transpose(0, 2, 1, 3).reshape(tok_rows, lin_heads_here, VAL_DIM)
    lin_out = head_norm(linear_rows, lin_gain.reshape(lin_heads_here, VAL_DIM)).astype(jnp.bfloat16)
    lin_out = lin_out.reshape(tok_rows, lin_heads_here * VAL_DIM)
    mixed = summed_on_arrival(
        (
            jnp.dot(diff_out, w_out_diff, preferred_element_type=jnp.float32)
            + jnp.dot(lin_out, w_out_lin, preferred_element_type=jnp.float32)
        ).astype(jnp.bfloat16),
        "tp",
        0,
    )
    return mixed.astype(jnp.bfloat16)


def solution(mesh):
    finer = Mesh(mesh.devices.reshape(8, 4, 2, mesh.shape["tp"]), ("sp_0", "sp_1", "sp_2", "tp"))
    in_specs = (
        P(SP, "tp"),
        P(SP, "tp"),
        P(SP, "tp"),
        P("tp"),
        P(),
        P(SP, "tp"),
        P(SP, "tp"),
        P(SP, "tp"),
        P(SP, "tp"),
        P("tp"),
        P("tp", None),
        P("tp", None),
    )
    out_specs = P(SP_TP, None)
    return jax.shard_map(body, mesh=finer, in_specs=in_specs, out_specs=out_specs, check_vma=False)
```

profile of v0, /device:TPU:225, one launch (start us, length us, event | category | flops | bytes accessed | tf_op | source)
XLA Modules:
  0.0 305.2 jit_solution(15642784460107298665)
XLA Ops:
  13.2 12.5 %while.55 = (s32[]{:T(128)}, f32[1,128,256]{2,1,0:T(8,128)S(1)}, f32[1,128]{1,0:T(1,128)S(1)}, f32[4,1,64,256]{3,2,1,0:T(8,128)S(1)}, bf16[4,1,64,128]{3,2,1,0:T...) while((s32[]{:T(128)}, f32[1,128,256]{2,1,0:T(8,128)S(1)}, ...), condition=%wide.region_15.16_spmd.clone, body=%wide.region_13.15_spmd.clone.sunk | while | flops 14336259 | bytes 5971633 | solution.py:196
  25.8 2.3 all-gather.2
  28.1 8.0 %all_gather.38 = bf16[4,1,128]{2,1,0:T(2,128)(2,1)S(1)} all-gather(bf16[1,1,128]{2,1,0:T(2,128)(2,1)S(1)} %get-tuple-element.692), channel_id=1, replica_groups=mesh['sp_0'=8,'sp_1'=4,'sp_2'=2,'tp'=4] {'sp_1'}, dimensions={0}, use_global_device_ids=true | all-gather | bytes 1280 | tf_op jit(solution)/shard_map/all_gather | solution.py:41
  36.0 10.5 %all_gather.39 = bf16[8,1,128]{2,1,0:T(2,128)(2,1)S(1)} all-gather(bf16[1,1,128]{2,1,0:T(2,128)(2,1)S(1)} %get-tuple-element.685), channel_id=1, replica_groups=mesh['sp_0'=8,'sp_1'=4,'sp_2'=2,'tp'=4] {'sp_0'}, dimensions={0}, use_global_device_ids=true | all-gather | bytes 2304 | tf_op jit(solution)/shard_map/all_gather | solution.py:41
  46.6 6.5 %all-gather.1 = bf16[2,128,256]{2,1,0:T(8,128)(2,1)S(1)} all-gather(bf16[1,128,256]{2,1,0:T(8,128)(2,1)S(1)} %convert_element_type.606), channel_id=3, replica_groups=mesh['sp_0'=8,'sp_1'=4,'sp_2'=2,'tp'=4] {'sp_2'}, dimensions={0}, use_global_device_ids=true | all-gather | bytes 196608 | tf_op jit(solution)/shard_map/all_gather | solution.py:41
  53.1 9.8 %all_gather.42 = bf16[4,1,128,256]{3,2,1,0:T(8,128)(2,1)S(1)} all-gather(bf16[1,1,128,256]{3,2,1,0:T(8,128)(2,1)S(1)} %fusion.110), channel_id=1, replica_groups=mesh['sp_0'=8,'sp_1'=4,'sp_2'=2,'tp'=4] {'sp_1'}, dimensions={0}, use_global_device_ids=true | all-gather | bytes 327680 | tf_op jit(solution)/shard_map/all_gather | solution.py:41
  63.1 25.3 %all_gather.43 = bf16[8,1,128,256]{3,2,1,0:T(8,128)(2,1)S(1)} all-gather(bf16[1,1,128,256]{3,2,1,0:T(8,128)(2,1)S(1)} %fusion.104), channel_id=1, replica_groups=mesh['sp_0'=8,'sp_1'=4,'sp_2'=2,'tp'=4] {'sp_0'}, dimensions={0}, use_global_device_ids=true | all-gather | bytes 589824 | tf_op jit(solution)/shard_map/all_gather | solution.py:41
  90.3 12.7 %all-gather.6.cloned.1.call-done = bf16[16384,1,384]{2,0,1:T(8,128)(2,1)} async-done(((bf16[256,1,384]{2,0,1:T(8,128)(2,1)}), bf16[16384,1,384]{2,0,1:T(8,128)(2,1)}) %all-gather.6.cloned.1.call-update) | async-done | bytes 12582928 | tf_op jit(solution)/shard_map/all_gather | solution.py:25
  103.0 7.0 %split.17 = bf16[16384,1,256]{2,0,1:T(8,128)(2,1)} slice(bf16[16384,1,384]{2,0,1:T(8,128)(2,1)} %all-gather.6.cloned.1.call-done), slice={[0:16384], [0:1], [128:384]} | slice | bytes 16777216 | tf_op jit(solution)/shard_map/split | solution.py:26
  110.0 3.8 %split.16 = bf16[16384,1,128]{2,0,1:T(8,128)(2,1)} slice(bf16[16384,1,384]{2,0,1:T(8,128)(2,1)} %all-gather.6.cloned.1.call-done), slice={[0:16384], [0:1], [0:128]} | slice | bytes 8388608 | tf_op jit(solution)/shard_map/split | solution.py:26
  113.8 56.2 %while.53 = (s32[]{:T(128)}, f32[1,2,256]{2,1,0:T(2,128)S(1)}, f32[1,2,256]{2,1,0:T(2,128)S(1)}, f32[1,2,256,256]{3,2,1,0:T(8,128)S(1)}, s32[]{:T(128)}, /*index...) while((s32[]{:T(128)}, f32[1,2,256]{2,1,0:T(2,128)S(1)}, ...), condition=%wide.region_5.6_spmd.clone, body=%wide.region_0.5_spmd.clone.sunk | while | flops 819728128 | bytes 17502528 | solution.py:115
  114.4 6.4 %conditional.6 = ((f32[1,2,256]{2,1,0:T(2,128)S(1)}, f32[1,2,256]{2,1,0:T(2,128)S(1)}, f32[1,2,256,256]{3,2,1,0:T(8,128)S(1)})) conditional(s32[]{:T(128)} %convert_element_type.912, (f32[1,2,256]{2,1,0:T(2,128)S(1)}, f32[1,2,256]{2,1,0:T(2,128)S(1)}, f32[1,2,256,256]{3,2,1,0:T(8,128)S(1)}) %tuple.128, (s32[]{:T(128)}, s32[]{:T(128)}, ...), branch_computations={%region_1.0_spmd, %region_2.4_spmd} | conditional | flops 819728128 | bytes 17493074 | solution.py:113
  115.0 1.8 fusion.4
  116.8 3.0 fusion.13
  121.5 6.4 %conditional.6 = ((f32[1,2,256]{2,1,0:T(2,128)S(1)}, f32[1,2,256]{2,1,0:T(2,128)S(1)}, f32[1,2,256,256]{3,2,1,0:T(8,128)S(1)})) conditional(s32[]{:T(128)} %convert_element_type.912, (f32[1,2,256]{2,1,0:T(2,128)S(1)}, f32[1,2,256]{2,1,0:T(2,128)S(1)}, f32[1,2,256,256]{3,2,1,0:T(8,128)S(1)}) %tuple.128, (s32[]{:T(128)}, s32[]{:T(128)}, ...), branch_computations={%region_1.0_spmd, %region_2.4_spmd} | conditional | flops 819728128 | bytes 17493074 | solution.py:113
  122.0 1.8 fusion.4
  123.8 2.9 fusion.13
  128.5 6.4 %conditional.6 = ((f32[1,2,256]{2,1,0:T(2,128)S(1)}, f32[1,2,256]{2,1,0:T(2,128)S(1)}, f32[1,2,256,256]{3,2,1,0:T(8,128)S(1)})) conditional(s32[]{:T(128)} %convert_element_type.912, (f32[1,2,256]{2,1,0:T(2,128)S(1)}, f32[1,2,256]{2,1,0:T(2,128)S(1)}, f32[1,2,256,256]{3,2,1,0:T(8,128)S(1)}) %tuple.128, (s32[]{:T(128)}, s32[]{:T(128)}, ...), branch_computations={%region_1.0_spmd, %region_2.4_spmd} | conditional | flops 819728128 | bytes 17493074 | solution.py:113
  129.0 1.8 fusion.4
  130.8 2.9 fusion.13
  135.5 6.4 %conditional.6 = ((f32[1,2,256]{2,1,0:T(2,128)S(1)}, f32[1,2,256]{2,1,0:T(2,128)S(1)}, f32[1,2,256,256]{3,2,1,0:T(8,128)S(1)})) conditional(s32[]{:T(128)} %convert_element_type.912, (f32[1,2,256]{2,1,0:T(2,128)S(1)}, f32[1,2,256]{2,1,0:T(2,128)S(1)}, f32[1,2,256,256]{3,2,1,0:T(8,128)S(1)}) %tuple.128, (s32[]{:T(128)}, s32[]{:T(128)}, ...), branch_computations={%region_1.0_spmd, %region_2.4_spmd} | conditional | flops 819728128 | bytes 17493074 | solution.py:113
  136.0 1.8 fusion.4
  137.8 2.9 fusion.13
  142.5 6.4 %conditional.6 = ((f32[1,2,256]{2,1,0:T(2,128)S(1)}, f32[1,2,256]{2,1,0:T(2,128)S(1)}, f32[1,2,256,256]{3,2,1,0:T(8,128)S(1)})) conditional(s32[]{:T(128)} %convert_element_type.912, (f32[1,2,256]{2,1,0:T(2,128)S(1)}, f32[1,2,256]{2,1,0:T(2,128)S(1)}, f32[1,2,256,256]{3,2,1,0:T(8,128)S(1)}) %tuple.128, (s32[]{:T(128)}, s32[]{:T(128)}, ...), branch_computations={%region_1.0_spmd, %region_2.4_spmd} | conditional | flops 819728128 | bytes 17493074 | solution.py:113
  143.0 1.8 fusion.4
  144.8 2.9 fusion.13
  149.5 6.4 %conditional.6 = ((f32[1,2,256]{2,1,0:T(2,128)S(1)}, f32[1,2,256]{2,1,0:T(2,128)S(1)}, f32[1,2,256,256]{3,2,1,0:T(8,128)S(1)})) conditional(s32[]{:T(128)} %convert_element_type.912, (f32[1,2,256]{2,1,0:T(2,128)S(1)}, f32[1,2,256]{2,1,0:T(2,128)S(1)}, f32[1,2,256,256]{3,2,1,0:T(8,128)S(1)}) %tuple.128, (s32[]{:T(128)}, s32[]{:T(128)}, ...), branch_computations={%region_1.0_spmd, %region_2.4_spmd} | conditional | flops 819728128 | bytes 17493074 | solution.py:113
  150.0 1.8 fusion.4
  151.8 2.9 fusion.13
  156.5 6.4 %conditional.6 = ((f32[1,2,256]{2,1,0:T(2,128)S(1)}, f32[1,2,256]{2,1,0:T(2,128)S(1)}, f32[1,2,256,256]{3,2,1,0:T(8,128)S(1)})) conditional(s32[]{:T(128)} %convert_element_type.912, (f32[1,2,256]{2,1,0:T(2,128)S(1)}, f32[1,2,256]{2,1,0:T(2,128)S(1)}, f32[1,2,256,256]{3,2,1,0:T(8,128)S(1)}) %tuple.128, (s32[]{:T(128)}, s32[]{:T(128)}, ...), branch_computations={%region_1.0_spmd, %region_2.4_spmd} | conditional | flops 819728128 | bytes 17493074 | solution.py:113
  157.0 1.8 fusion.4
  158.8 2.9 fusion.13
  163.5 6.5 %conditional.6 = ((f32[1,2,256]{2,1,0:T(2,128)S(1)}, f32[1,2,256]{2,1,0:T(2,128)S(1)}, f32[1,2,256,256]{3,2,1,0:T(8,128)S(1)})) conditional(s32[]{:T(128)} %convert_element_type.912, (f32[1,2,256]{2,1,0:T(2,128)S(1)}, f32[1,2,256]{2,1,0:T(2,128)S(1)}, f32[1,2,256,256]{3,2,1,0:T(8,128)S(1)}) %tuple.128, (s32[]{:T(128)}, s32[]{:T(128)}, ...), branch_computations={%region_1.0_spmd, %region_2.4_spmd} | conditional | flops 819728128 | bytes 17493074 | solution.py:113
  164.0 1.8 fusion.4
  165.8 3.0 fusion.13
  170.2 22.0 %all-gather.8.cloned.1.call-done = bf16[16384,1,384]{2,0,1:T(8,128)(2,1)} async-done(((bf16[256,1,384]{2,0,1:T(8,128)(2,1)}), bf16[16384,1,384]{2,0,1:T(8,128)(2,1)}) %all-gather.8.cloned.1.call-update) | async-done | bytes 12582928 | tf_op jit(solution)/shard_map/all_gather | solution.py:25
  192.2 7.0 %split.19 = bf16[16384,1,256]{2,0,1:T(8,128)(2,1)} slice(bf16[16384,1,384]{2,0,1:T(8,128)(2,1)} %all-gather.8.cloned.1.call-done), slice={[0:16384], [0:1], [128:384]} | slice | bytes 16777216 | tf_op jit(solution)/shard_map/split | solution.py:26
  199.3 3.7 %split.18 = bf16[16384,1,128]{2,0,1:T(8,128)(2,1)} slice(bf16[16384,1,384]{2,0,1:T(8,128)(2,1)} %all-gather.8.cloned.1.call-done), slice={[0:16384], [0:1], [0:128]} | slice | bytes 8388608 | tf_op jit(solution)/shard_map/split | solution.py:26
  203.1 56.0 %while.54 = (s32[]{:T(128)}, f32[1,2,256]{2,1,0:T(2,128)S(1)}, f32[1,2,256]{2,1,0:T(2,128)S(1)}, f32[1,2,256,256]{3,2,1,0:T(8,128)S(1)}, s32[]{:T(128)}, /*index...) while((s32[]{:T(128)}, f32[1,2,256]{2,1,0:T(2,128)S(1)}, ...), condition=%wide.region_11.12_spmd.clone, body=%wide.region_6.11_spmd.clone.sunk | while | flops 819728128 | bytes 17502528 | solution.py:115
  203.7 6.4 %conditional.7 = ((f32[1,2,256]{2,1,0:T(2,128)S(1)}, f32[1,2,256]{2,1,0:T(2,128)S(1)}, f32[1,2,256,256]{3,2,1,0:T(8,128)S(1)})) conditional(s32[]{:T(128)} %convert_element_type.913, (f32[1,2,256]{2,1,0:T(2,128)S(1)}, f32[1,2,256]{2,1,0:T(2,128)S(1)}, f32[1,2,256,256]{3,2,1,0:T(8,128)S(1)}) %tuple.131, (s32[]{:T(128)}, s32[]{:T(128)}, ...), branch_computations={%region_7.7_spmd, %region_8.10_spmd} | conditional | flops 819728128 | bytes 17493074 | solution.py:113
  206.0 2.9 fusion.37
  210.6 6.4 %conditional.7 = ((f32[1,2,256]{2,1,0:T(2,128)S(1)}, f32[1,2,256]{2,1,0:T(2,128)S(1)}, f32[1,2,256,256]{3,2,1,0:T(8,128)S(1)})) conditional(s32[]{:T(128)} %convert_element_type.913, (f32[1,2,256]{2,1,0:T(2,128)S(1)}, f32[1,2,256]{2,1,0:T(2,128)S(1)}, f32[1,2,256,256]{3,2,1,0:T(8,128)S(1)}) %tuple.131, (s32[]{:T(128)}, s32[]{:T(128)}, ...), branch_computations={%region_7.7_spmd, %region_8.10_spmd} | conditional | flops 819728128 | bytes 17493074 | solution.py:113
  211.2 1.8 fusion.28
  213.0 2.9 fusion.37
  217.6 6.4 %conditional.7 = ((f32[1,2,256]{2,1,0:T(2,128)S(1)}, f32[1,2,256]{2,1,0:T(2,128)S(1)}, f32[1,2,256,256]{3,2,1,0:T(8,128)S(1)})) conditional(s32[]{:T(128)} %convert_element_type.913, (f32[1,2,256]{2,1,0:T(2,128)S(1)}, f32[1,2,256]{2,1,0:T(2,128)S(1)}, f32[1,2,256,256]{3,2,1,0:T(8,128)S(1)}) %tuple.131, (s32[]{:T(128)}, s32[]{:T(128)}, ...), branch_computations={%region_7.7_spmd, %region_8.10_spmd} | conditional | flops 819728128 | bytes 17493074 | solution.py:113
  218.2 1.8 fusion.28
  220.0 2.9 fusion.37
  224.6 6.4 %conditional.7 = ((f32[1,2,256]{2,1,0:T(2,128)S(1)}, f32[1,2,256]{2,1,0:T(2,128)S(1)}, f32[1,2,256,256]{3,2,1,0:T(8,128)S(1)})) conditional(s32[]{:T(128)} %convert_element_type.913, (f32[1,2,256]{2,1,0:T(2,128)S(1)}, f32[1,2,256]{2,1,0:T(2,128)S(1)}, f32[1,2,256,256]{3,2,1,0:T(8,128)S(1)}) %tuple.131, (s32[]{:T(128)}, s32[]{:T(128)}, ...), branch_computations={%region_7.7_spmd, %region_8.10_spmd} | conditional | flops 819728128 | bytes 17493074 | solution.py:113
  225.2 1.8 fusion.28
  227.0 2.9 fusion.37
  231.6 6.4 %conditional.7 = ((f32[1,2,256]{2,1,0:T(2,128)S(1)}, f32[1,2,256]{2,1,0:T(2,128)S(1)}, f32[1,2,256,256]{3,2,1,0:T(8,128)S(1)})) conditional(s32[]{:T(128)} %convert_element_type.913, (f32[1,2,256]{2,1,0:T(2,128)S(1)}, f32[1,2,256]{2,1,0:T(2,128)S(1)}, f32[1,2,256,256]{3,2,1,0:T(8,128)S(1)}) %tuple.131, (s32[]{:T(128)}, s32[]{:T(128)}, ...), branch_computations={%region_7.7_spmd, %region_8.10_spmd} | conditional | flops 819728128 | bytes 17493074 | solution.py:113
  232.2 1.8 fusion.28
  234.0 2.9 fusion.37
  238.6 6.4 %conditional.7 = ((f32[1,2,256]{2,1,0:T(2,128)S(1)}, f32[1,2,256]{2,1,0:T(2,128)S(1)}, f32[1,2,256,256]{3,2,1,0:T(8,128)S(1)})) conditional(s32[]{:T(128)} %convert_element_type.913, (f32[1,2,256]{2,1,0:T(2,128)S(1)}, f32[1,2,256]{2,1,0:T(2,128)S(1)}, f32[1,2,256,256]{3,2,1,0:T(8,128)S(1)}) %tuple.131, (s32[]{:T(128)}, s32[]{:T(128)}, ...), branch_computations={%region_7.7_spmd, %region_8.10_spmd} | conditional | flops 819728128 | bytes 17493074 | solution.py:113
  239.1 1.8 fusion.28
  241.0 2.9 fusion.37
  245.6 6.4 %conditional.7 = ((f32[1,2,256]{2,1,0:T(2,128)S(1)}, f32[1,2,256]{2,1,0:T(2,128)S(1)}, f32[1,2,256,256]{3,2,1,0:T(8,128)S(1)})) conditional(s32[]{:T(128)} %convert_element_type.913, (f32[1,2,256]{2,1,0:T(2,128)S(1)}, f32[1,2,256]{2,1,0:T(2,128)S(1)}, f32[1,2,256,256]{3,2,1,0:T(8,128)S(1)}) %tuple.131, (s32[]{:T(128)}, s32[]{:T(128)}, ...), branch_computations={%region_7.7_spmd, %region_8.10_spmd} | conditional | flops 819728128 | bytes 17493074 | solution.py:113
  246.1 1.8 fusion.28
  248.0 2.9 fusion.37
  252.6 6.4 %conditional.7 = ((f32[1,2,256]{2,1,0:T(2,128)S(1)}, f32[1,2,256]{2,1,0:T(2,128)S(1)}, f32[1,2,256,256]{3,2,1,0:T(8,128)S(1)})) conditional(s32[]{:T(128)} %convert_element_type.913, (f32[1,2,256]{2,1,0:T(2,128)S(1)}, f32[1,2,256]{2,1,0:T(2,128)S(1)}, f32[1,2,256,256]{3,2,1,0:T(8,128)S(1)}) %tuple.131, (s32[]{:T(128)}, s32[]{:T(128)}, ...), branch_computations={%region_7.7_spmd, %region_8.10_spmd} | conditional | flops 819728128 | bytes 17493074 | solution.py:113
  255.0 2.9 fusion.37
  261.4 3.5 %fusion.204 = f32[256,4096]{1,0:T(8,128)S(1)} fusion(bf16[256,512]{0,1:T(8,128)(2,1)S(1)} %bitcast.450, bf16[512,4096]{1,0:T(8,128)(2,1)} %param.32), kind=kOutput, calls=%fused_computation.287 | convolution fusion | flops 1073741824 | bytes 8650752 | tf_op jit(solution)/shard_map/dot_general | solution.py:215
  265.8 29.8 %all_to_all.5 = bf16[4,64,4096]{2,1,0:T(8,128)(2,1)} all-to-all(bf16[4,64,4096]{2,1,0:T(8,128)(2,1)S(1)} %bitcast.449), channel_id=1, replica_groups=mesh['sp_0'=8,'sp_1'=4,'sp_2'=2,'tp'=4] {'tp'}, dimensions={0} | all-to-all | bytes 4194304 | tf_op jit(solution)/shard_map/all_to_all | solution.py:64
  295.5 2.9 reduce_sum.54
  (265 shorter events, 53.6 us)
Async XLA Ops:
  6.5 258.4 %copy-start = (bf16[256,4096]{1,0:T(8,128)(2,1)S(1)}, bf16[256,4096]{1,0:T(8,128)(2,1)}, u32[]{:S(2)}) copy-start(bf16[256,4096]{1,0:T(8,128)(2,1)} %param.33) | copy-start | bytes 6291460
  6.5 96.4 %all-gather.6.cloned.1.call-start = ((), (), s32[]{:S(2)}) async-start(), calls=%async_computation.1 | async-start | bytes 12779520 | tf_op jit(solution)/shard_map/all_gather | solution.py:25
  9.7 182.6 %all-gather.8.cloned.1.call-start = ((), (), s32[]{:S(2)}) async-start(), calls=%async_computation.2 | async-start | bytes 12779520 | tf_op jit(solution)/shard_map/all_gather | solution.py:25
  13.2 2.5 copy-start.2
  16.3 2.5 copy-start.2
  19.5 2.5 copy-start.2
  22.6 2.5 copy-start.2
  25.7 64.0 %copy-start.3 = (bf16[256,512]{1,0:T(8,128)(2,1)S(1)}, bf16[256,512]{1,0:T(8,128)(2,1)}, u32[]{:S(2)}) copy-start(bf16[256,512]{1,0:T(8,128)(2,1)} %param.22) | copy-start | bytes 786436
  25.7 64.4 %copy-start.4 = (f32[256]{0:T(256)S(1)}, f32[256]{0:T(256)}, u32[]{:S(2)}) copy-start(f32[256]{0:T(256)} %param.31) | copy-start | bytes 3076
  203.0 58.1 %copy-start.6 = (f32[2]{0:T(128)S(1)}, f32[2]{0:T(128)}, u32[]{:S(2)}) copy-start(f32[2]{0:T(128)} %param.25) | copy-start | bytes 28
  203.0 58.3 %copy-start.5 = (f32[256]{0:T(256)S(1)}, f32[256]{0:T(256)}, u32[]{:S(2)}) copy-start(f32[256]{0:T(256)} %param.26) | copy-start | bytes 3076
  259.0 0.8 copy-start.1
Sparse Core Ops, SparseCore 0:
  10.1 92.8 all-gather.5
  105.7 86.4 all-gather.7
where the time goes:
time: 308 us; the launch traced here: 305 us
  blocking collectives  92 us (30%)
  matrix products  82.9 us (27%)
  other arithmetic  43.4 us (14%)
  waiting for transfers between devices  35.4 us (11%)
  local copies, waits for them, and re-layouts  26.6 us (9%)
  between operations  13.8 us (4%)
  loops' own time  11.1 us (4%)
    all_gather x6, blocking collectives, entering(): lax.all_gather(part.astype(kind), axis)  62.2 us
    dot_general x16, matrix products, compute(): jnp.einsum('gjqs,sge->gjqe', weights.astype(jnp.bfloat16), value_part, pr...  46.9 us
    all_gather x2, waiting for transfers between devices, side_by_side(): out = lax.all_gather(both, axis, axis=dim, tiled=True)  34.7 us
    all_to_all x1, blocking collectives, summed_on_arrival(): lax.all_to_all(blocks, axis, split_axis=0, concat_axis=0, tiled=True)  29.8 us
    dot_general x16, matrix products, compute(): jnp.einsum('gjqd,sgd->gjqs', query_map, key_part, preferred_element_type=...  28.8 us
    split x4, local copies, waits for them, and re-layouts, side_by_side(): jnp.split(out, [sum(widths[:k]) for k in range(1, len(widths))], axis=along)  21.5 us
    reduce_sum x16, other arithmetic, compute(): new_total = old_total * shrink + jnp.sum(weights, axis=-1)  17.7 us
    another operation x2, loops' own time, attend(): return lax.fori_loop(0, row_count // step_rows, visit, carries)  9.6 us
  transfers between devices with their start and end apart: 2, of which 2 were waited for; matrix products, arithmetic and copies ran while one was open for 26% of the time, Pallas kernels for 0%

commit v1 on v0

v1 whole, which is shorter than its diff:
```python
import functools
import math

import jax
import jax.numpy as jnp
from jax import lax
from jax.experimental import pallas as pl
from jax.experimental.pallas import tpu as pltpu
from jax.sharding import Mesh
from jax.sharding import PartitionSpec as P

HEAD_DIM = 128
KEY_DIM = 128
VAL_DIM = 256
BLOCK = 64
SP = ("sp_0", "sp_1", "sp_2")
CHIPS = ("sp_0", "sp_1")
SP_TP = ("sp_0", "sp_1", "sp_2", "tp")

norm_eps = 1e-06
gate_temp = 16.0
neg_large = -1e30
HIGHEST = lax.Precision.HIGHEST
SCORE_SCALE = math.log2(math.e) / math.sqrt(HEAD_DIM)


def head_norm(mixed_in, gain):
    return (
        mixed_in
        * lax.rsqrt(jnp.mean(mixed_in * mixed_in, axis=-1, keepdims=True) + norm_eps)
        * gain
    )


def dot_nt(a, b, precision=None):
    return lax.dot_general(
        a, b, (((1,), (1,)), ((), ())), precision=precision, preferred_element_type=jnp.float32
    )


def dot_tn(a, b, precision=None):
    return lax.dot_general(
        a, b, (((0,), (0,)), ((), ())), precision=precision, preferred_element_type=jnp.float32
    )


def linear_kernel(q_ref, k_ref, v_ref, decay_ref, local_ref, reach_ref, state_ref, total_ref):
    rows = lax.broadcasted_iota(jnp.int32, (BLOCK, BLOCK), 0)
    cols = lax.broadcasted_iota(jnp.int32, (BLOCK, BLOCK), 1)
    lower = rows >= cols
    ones = jnp.where(lower, 1.0, 0.0)
    passed = jnp.zeros((1, KEY_DIM), jnp.float32)
    state = jnp.zeros((KEY_DIM, VAL_DIM), jnp.float32)
    for index in range(q_ref.shape[0] // BLOCK):
        part = slice(index * BLOCK, (index + 1) * BLOCK)
        pre = decay_ref[part, :]
        log_decay = (jnp.minimum(pre, 0.0) - jnp.log1p(jnp.exp(-jnp.abs(pre)))) / gate_temp
        cumulative = jnp.dot(ones, log_decay, precision=HIGHEST, preferred_element_type=jnp.float32)
        query = q_ref[part, :].astype(jnp.float32) * (KEY_DIM**-0.5)
        key = k_ref[part, :].astype(jnp.float32)
        value = v_ref[part, :].astype(jnp.float32)
        query_decayed = query * jnp.exp(cumulative)
        inner = dot_nt(query_decayed, key * jnp.exp(-cumulative), HIGHEST)
        inner = jnp.where(lower, inner, 0.0)
        local = jnp.dot(inner, value, precision=HIGHEST, preferred_element_type=jnp.float32)
        local_ref[part, :] = local + jnp.dot(
            query_decayed, state, precision=HIGHEST, preferred_element_type=jnp.float32
        )
        reach_ref[part, :] = query_decayed * jnp.exp(passed)
        last = cumulative[BLOCK - 1 :, :]
        shrink = jnp.transpose(jnp.broadcast_to(jnp.exp(last), (8, KEY_DIM)))[:, :1]
        state = shrink * state + dot_tn(key * jnp.exp(last - cumulative), value, HIGHEST)
        passed = passed + last
    state_ref[...] = state
    total_ref[...] = jnp.broadcast_to(passed, (8, KEY_DIM))


def absorb(q2_ref, keys, values, top_ref, total_ref, numer_ref, group, hidden):
    scores = dot_nt(q2_ref[group], jnp.concatenate([keys, keys], axis=1))
    if hidden is not None:
        scores = jnp.where(hidden, 2 * neg_large, scores)
    old_top = top_ref[group][:, :1]
    new_top = jnp.maximum(old_top, jnp.max(scores, axis=1, keepdims=True))
    weights = jnp.exp2(scores - new_top)
    shrink = jnp.exp2(old_top - new_top)
    folded = weights[:, :128]
    for tile in range(1, weights.shape[1] // 128):
        folded = folded + weights[:, tile * 128 : (tile + 1) * 128]
    total_ref[group] = total_ref[group] * shrink + folded
    top_ref[group] = jnp.broadcast_to(new_top, (new_top.shape[0], 128))
    numer_ref[group] = numer_ref[group] * shrink + jnp.dot(
        weights.astype(jnp.bfloat16), values, preferred_element_type=jnp.float32
    )


FIRST = 160
SECOND = 96
Z, Y = 8, 4
MESH_IDS = pl.DeviceIdType.MESH
KEY_COLS = slice(0, 2 * HEAD_DIM)
VALUE_COLS = slice(2 * HEAD_DIM, 2 * HEAD_DIM + VAL_DIM)


def remote(src, dst, send, recv, **where):
    return pltpu.make_async_remote_copy(
        src_ref=src,
        dst_ref=dst,
        send_sem=send,
        recv_sem=recv,
        device_id=where,
        device_id_type=MESH_IDS,
    )


def as_column(row):
    return jnp.transpose(jnp.broadcast_to(row, (8, KEY_DIM)))[:, :1]


def mixer_kernel(
    q_hbm,
    k_hbm,
    v_hbm,
    lam_ref,
    diff_gain_ref,
    lin_q_ref,
    lin_k_ref,
    lin_v_ref,
    decay_ref,
    lin_gain_ref,
    act_ref,
    kva,
    kvb,
    both_q,
    q2_ref,
    top_ref,
    total_ref,
    numer_ref,
    stat_ref,
    far_stat,
    far_numer,
    local_ref,
    reach_ref,
    core_state,
    core_decay,
    chip_state,
    chip_decay,
    chain_ref,
    own_sems,
    recv_a,
    recv_b,
    send_az,
    send_ay,
    send_af,
    send_by,
    send_bf,
    send_bz,
    pair_send,
    pair_recv,
    line_send,
    line_recv,
    chain_send,
    chain_recv,
):
    z, y, core = (lax.axis_index(name) for name in SP)
    tok_rows = q_hbm.shape[0]
    chip_rows = 2 * tok_rows
    up, down = lax.rem(z + 1, Z), lax.rem(z + Z - 1, Z)
    east, west = lax.rem(y + 1, Y), lax.rem(y + Y - 1, Y)
    across = lax.rem(y + 2, Y)
    other = 1 - core

    owned = [
        pltpu.make_async_copy(
            k_hbm.at[pl.ds(0, FIRST)], kva.at[z, y, :, KEY_COLS], own_sems.at[0]
        ),
        pltpu.make_async_copy(
            v_hbm.at[pl.ds(0, FIRST)], kva.at[z, y, :, VALUE_COLS], own_sems.at[1]
        ),
        pltpu.make_async_copy(
            k_hbm.at[pl.ds(FIRST, SECOND)], kvb.at[z, y, :, KEY_COLS], own_sems.at[2]
        ),
        pltpu.make_async_copy(
            v_hbm.at[pl.ds(FIRST, SECOND)], kvb.at[z, y, :, VALUE_COLS], own_sems.at[3]
        ),
        pltpu.make_async_copy(q_hbm, both_q.at[core], own_sems.at[4]),
    ]
    for copy in owned:
        copy.start()
    barrier = pltpu.get_barrier_semaphore()
    for where in (
        {"sp_0": up},
        {"sp_0": down},
        {"sp_1": east},
        {"sp_1": west},
        {"sp_1": across},
        {"sp_2": other},
    ):
        pl.semaphore_signal(barrier, inc=1, device_id=where, device_id_type=MESH_IDS)
    pl.semaphore_wait(barrier, 6)
    for copy in owned:
        copy.wait()

    def a_z(zo, toward, way, cols=slice(None), half=0):
        block = kva.at[zo, y, :, cols]
        return remote(block, block, send_az.at[zo, way], recv_a.at[zo, y, half], sp_0=toward)

    def a_y(zo, toward, way):
        block = kva.at[zo, y]
        return remote(block, block, send_ay.at[zo, way], recv_a.at[zo, y, 0], sp_1=toward)

    def a_far(zo, yo, toward, way):
        block = kva.at[zo, yo, :, (KEY_COLS, VALUE_COLS)[way]]
        return remote(block, block, send_af.at[zo, way], recv_a.at[zo, yo, way], sp_1=toward)

    def a_wait(zo, yo, cols=slice(None), half=0):
        block = kva.at[zo, yo, :, cols]
        remote(block, block, send_az.at[zo, 0], recv_a.at[zo, yo, half], sp_0=up).wait_recv()

    def b_y(toward, way):
        block = kvb.at[z, y]
        return remote(block, block, send_by.at[way], recv_b.at[z, y, 0], sp_1=toward)

    def b_far(yo, toward, way):
        block = kvb.at[z, yo, :, (KEY_COLS, VALUE_COLS)[way]]
        return remote(block, block, send_bf.at[way], recv_b.at[z, yo, way], sp_1=toward)

    def b_z(zo, yo, toward, way, cols=slice(None), half=0):
        block = kvb.at[zo, yo, :, cols]
        return remote(block, block, send_bz.at[zo, yo, way], recv_b.at[zo, yo, half], sp_0=toward)

    def b_wait(zo, yo, cols=slice(None), half=0):
        block = kvb.at[zo, yo, :, cols]
        remote(block, block, send_bz.at[zo, yo, 0], recv_b.at[zo, yo, half], sp_0=up).wait_recv()

    pair_q = remote(
        both_q.at[core], both_q.at[core], pair_send.at[0], pair_recv.at[0], sp_2=other
    )
    pair_q.start()
    a_z(z, up, 0).start()
    a_z(z, down, 1).start()
    b_y(east, 0).start()
    b_y(west, 1).start()
    a_y(z, east, 0).start()
    a_y(z, west, 1).start()
    b_z(z, y, up, 0).start()
    b_z(z, y, down, 1).start()

    linear_kernel(
        lin_q_ref,
        lin_k_ref,
        lin_v_ref,
        decay_ref,
        local_ref,
        reach_ref,
        core_state.at[core],
        core_decay.at[core],
    )
    pair_state = remote(
        core_state.at[core], core_state.at[core], pair_send.at[1], pair_recv.at[1], sp_2=other
    )
    pair_decay = remote(
        core_decay.at[core], core_decay.at[core], pair_send.at[2], pair_recv.at[2], sp_2=other
    )
    pair_state.start()
    pair_decay.start()

    b_wait(z, west)
    b_far(west, east, 0).start()
    b_z(z, west, up, 0).start()
    b_z(z, west, down, 1).start()
    b_wait(z, east)
    b_far(east, west, 1).start()
    b_z(z, east, up, 0).start()
    b_z(z, east, down, 1).start()

    top_ref[...] = jnp.full_like(top_ref, neg_large)
    total_ref[...] = jnp.zeros_like(total_ref)
    numer_ref[...] = jnp.zeros_like(numer_ref)
    pair_q.wait_recv()
    for group in range(4):
        mapping, head = group // 2, group % 2
        first = (head * 2 + mapping) * HEAD_DIM
        for side in range(2):
            scaled = both_q[side, :, first : first + HEAD_DIM].astype(jnp.float32) * SCORE_SCALE
            high = scaled.astype(jnp.bfloat16)
            low = (scaled - high.astype(jnp.float32)).astype(jnp.bfloat16)
            part = slice(side * tok_rows, (side + 1) * tok_rows)
            q2_ref[group, part, :HEAD_DIM] = high
            q2_ref[group, part, HEAD_DIM:] = low

    pair_state.wait_recv()
    pair_decay.wait_recv()
    chip_state[y] = (
        as_column(jnp.exp(core_decay[1][:1])) * core_state[0] + core_state[1]
    ).astype(jnp.bfloat16)
    chip_decay[y] = core_decay[0] + core_decay[1]

    b_wait(z, across, KEY_COLS, 0)
    b_wait(z, across, VALUE_COLS, 1)
    b_z(z, across, up, 0).start()
    b_z(z, across, down, 1).start()

    def line(peer, index):
        return (
            remote(
                chip_state.at[y],
                chip_state.at[y],
                line_send.at[index, 0],
                line_recv.at[y, 0],
                sp_1=peer,
            ),
            remote(
                chip_decay.at[y],
                chip_decay.at[y],
                line_send.at[index, 1],
                line_recv.at[y, 1],
                sp_1=peer,
            ),
        )

    for index, peer in enumerate((east, west, across)):
        for copy in line(peer, index):
            copy.start()

    def chain_copy():
        return remote(
            chain_ref.at[1], chain_ref.at[0], chain_send.at[0], chain_recv.at[0], sp_0=up
        )

    def follow(state, yo):
        return as_column(jnp.exp(chip_decay[yo][:1])) * state + chip_state[yo].astype(jnp.float32)

    def pass_on():
        state = chain_ref[0]
        for yo in range(Y):
            state = follow(state, yo)
        chain_ref[1] = state
        chain_copy().start()

    @pl.when(z == 0)
    def _():
        chain_ref[0] = jnp.zeros_like(chain_ref[0])

    order = lambda index: lax.rem(
        y + jnp.where(index == 0, 0, jnp.where(index == 1, Y - 1, jnp.where(index == 2, 1, 2))), Y
    )
    origin = lambda unit: lax.rem(
        z + 2 * Z + jnp.where(lax.rem(unit, 2) == 1, -((unit + 1) // 2), unit // 2), Z
    )

    def compute(store, zo, group, hidden):
        mapping = group // 2
        tokens = store.shape[2]
        first = pl.multiple_of(mapping * HEAD_DIM, HEAD_DIM)
        keys = store[zo, :, :, pl.ds(first, HEAD_DIM)].reshape(Y * tokens, HEAD_DIM)
        values = store[zo, :, :, VALUE_COLS].reshape(Y * tokens, VAL_DIM)
        absorb(q2_ref, keys, values, top_ref, total_ref, numer_ref, group, hidden)

    def hidden_from(tokens, start):
        column = lax.broadcasted_iota(jnp.int32, (chip_rows, Y * tokens), 1)
        row = lax.broadcasted_iota(jnp.int32, (chip_rows, Y * tokens), 0)
        chip = jnp.zeros_like(column)
        for index in range(1, Y):
            chip = chip + jnp.where(column >= index * tokens, 1, 0)
        key_pos = column + chip * (chip_rows - tokens) + core * tok_rows + start
        return key_pos > y * chip_rows + row

    def a_step(distance):
        for way, zo, toward in (
            (0, lax.rem(z + Z - distance, Z), up),
            (1, lax.rem(z + distance, Z), down),
        ):
            a_wait(zo, y)

            @pl.when(distance < 3)
            def _():
                a_z(zo, toward, way).start()

            @pl.when(distance == 3)
            def _():
                a_z(zo, toward, way, (KEY_COLS, VALUE_COLS)[way], way).start()

            a_y(zo, east, 0).start()
            a_y(zo, west, 1).start()

    def a_near(zo):
        a_wait(zo, west)
        a_far(zo, west, east, 0).start()
        a_wait(zo, east)
        a_far(zo, east, west, 1).start()

    def half_step(h, carry):
        @pl.when(h <= 2)
        def _():
            a_step(h + 1)

        @pl.when(h == 3)
        def _():
            zo = lax.rem(z + 4, Z)
            a_wait(zo, y, KEY_COLS, 0)
            a_wait(zo, y, VALUE_COLS, 1)
            a_y(zo, east, 0).start()
            a_y(zo, west, 1).start()

        @pl.when(h == 0)
        def _():
            a_near(z)

        @pl.when((h == 2) | (h == 4) | (h == 6))
        def _():
            a_near(lax.rem(z + Z - h // 2, Z))
            a_near(lax.rem(z + h // 2, Z))

        @pl.when(h == 8)
        def _():
            a_near(lax.rem(z + 4, Z))

        a_unit, b_unit = h - 2, h - 1
        a_origin, b_origin = origin(jnp.maximum(a_unit, 0)), origin(jnp.maximum(b_unit, 0))

        @pl.when(h >= 2)
        def _():
            a_wait(a_origin, across, KEY_COLS, 0)
            a_wait(a_origin, across, VALUE_COLS, 1)

        def piece(j, inner):
            distance = h // 2 + 1
            yo = order(lax.rem(h, 2) * 2 + j // 2)
            ahead, behind = lax.rem(z + Z - distance, Z), lax.rem(z + distance, Z)

            @pl.when((h <= 5) & (lax.rem(j, 2) == 0))
            def _():
                b_wait(ahead, yo)

                @pl.when(distance < 3)
                def _():
                    b_z(ahead, yo, up, 0).start()

                @pl.when(distance == 3)
                def _():
                    b_z(ahead, yo, up, 0, KEY_COLS, 0).start()

            @pl.when((h <= 5) & (lax.rem(j, 2) == 1))
            def _():
                b_wait(behind, yo)

                @pl.when(distance < 3)
                def _():
                    b_z(behind, yo, down, 1).start()

                @pl.when(distance == 3)
                def _():
                    b_z(behind, yo, down, 1, VALUE_COLS, 1).start()

            @pl.when(((h == 6) | (h == 7)) & (lax.rem(j, 2) == 1))
            def _():
                b_wait(ahead, yo, KEY_COLS, 0)
                b_wait(ahead, yo, VALUE_COLS, 1)

            slot = (h - 1) * 2 + j // 2

            @pl.when((h >= 1) & (lax.rem(j, 2) == 0) & (slot == z))
            def _():
                @pl.when(z > 0)
                def _():
                    chain_copy().wait_recv()

                @pl.when(z < Z - 1)
                def _():
                    pass_on()

            @pl.when((h >= 2) & (a_unit > 0) & (a_origin < z))
            def _():
                compute(kva, a_origin, j, None)

            @pl.when(a_unit == 0)
            def _():
                compute(kva, z, j, hidden_from(FIRST, 0))

            @pl.when((b_unit > 0) & (h <= 8) & (b_origin < z))
            def _():
                compute(kvb, b_origin, j, None)

            @pl.when(b_unit == 0)
            def _():
                compute(kvb, z, j, hidden_from(SECOND, FIRST))

            return inner

        @pl.when(h == 1)
        def _():
            for peer in (east, west, across):
                for part, buffer in enumerate((chip_state, chip_decay)):
                    remote(
                        buffer.at[peer],
                        buffer.at[peer],
                        line_send.at[0, part],
                        line_recv.at[peer, part],
                        sp_1=peer,
                    ).wait_recv()

        return lax.fori_loop(0, 4, piece, carry)

    lax.fori_loop(0, 10, half_step, 0)

    lane = lax.broadcasted_iota(jnp.int32, (chip_rows, 128), 1)
    for group in range(4):
        summed = jnp.sum(total_ref[group], axis=1, keepdims=True)
        stat_ref[group] = jnp.where(lane < 64, top_ref[group], summed)
    theirs = pl.ds(pl.multiple_of(other * tok_rows, tok_rows), tok_rows)
    mine = pl.ds(pl.multiple_of(core * tok_rows, tok_rows), tok_rows)
    swap_numer = remote(
        numer_ref.at[:, theirs], far_numer, pair_send.at[3], pair_recv.at[3], sp_2=other
    )
    swap_stat = remote(
        stat_ref.at[:, theirs], far_stat, pair_send.at[4], pair_recv.at[4], sp_2=other
    )
    swap_numer.start()
    swap_stat.start()

    state = chain_ref[0]
    for yo in range(Y - 1):
        state = jnp.where(yo < y, follow(state, yo), state)
    after = as_column(jnp.exp(core_decay[0][:1])) * state + core_state[0]
    state = jnp.where(core == 1, after, state)
    rows = local_ref[...] + jnp.dot(
        reach_ref[...], state, precision=HIGHEST, preferred_element_type=jnp.float32
    )
    act_ref[:, 2 * VAL_DIM :] = head_norm(rows, lin_gain_ref[...]).astype(act_ref.dtype)

    swap_numer.wait_recv()
    swap_stat.wait_recv()

    def merged(group):
        near, far = stat_ref[group, mine], far_stat[group]
        near_top, far_top = near[:, :1], far[:, :1]
        both_top = jnp.maximum(near_top, far_top)
        near_scale, far_scale = jnp.exp2(near_top - both_top), jnp.exp2(far_top - both_top)
        total = near[:, 64:65] * near_scale + far[:, 64:65] * far_scale
        numer = numer_ref[group, mine] * near_scale + far_numer[group] * far_scale
        return numer / total

    for head in range(2):
        attended = merged(head) - lam_ref[head] * merged(2 + head)
        act_ref[:, head * VAL_DIM : (head + 1) * VAL_DIM] = head_norm(
            attended, diff_gain_ref[...]
        ).astype(act_ref.dtype)

    for copy in (pair_q, pair_state, pair_decay, swap_numer, swap_stat):
        copy.wait_send()
    for index, peer in enumerate((east, west, across)):
        for copy in line(peer, index):
            copy.wait_send()

    @pl.when(z < Z - 1)
    def _():
        chain_copy().wait_send()

    for way, toward in ((0, east), (1, west)):
        b_y(toward, way).wait_send()
        b_far(west if way == 0 else east, toward, way).wait_send()

    def drain(offset, carry):
        zo = lax.rem(z + offset, Z)
        for way, toward in ((0, east), (1, west)):
            a_y(zo, toward, way).wait_send()
            a_far(zo, west if way == 0 else east, toward, way).wait_send()
        return carry

    lax.fori_loop(0, Z, drain, 0)
    for way, toward, sign, cols in ((0, up, -1, KEY_COLS), (1, down, 1, VALUE_COLS)):

        def drain_z(distance, carry):
            zo = lax.rem(z + Z + sign * distance, Z)
            a_z(zo, toward, way).wait_send()
            for yo in range(Y):
                b_z(zo, yo, toward, way).wait_send()
            return carry

        lax.fori_loop(0, 3, drain_z, 0)
        zo = lax.rem(z + Z + sign * 3, Z)
        a_z(zo, toward, way, cols, way).wait_send()
        for yo in range(Y):
            b_z(zo, yo, toward, way, cols, way).wait_send()


def mixer(
    queries, keys, values, lam, diff_gain, lin_query, lin_key, lin_value, decay_pre, lin_gain
):
    tok_rows = queries.shape[0]
    rows = 2 * tok_rows
    width = 2 * HEAD_DIM + VAL_DIM
    in_hbm = pl.BlockSpec(memory_space=pl.ANY)
    in_vmem = pl.BlockSpec(memory_space=pltpu.VMEM)
    dma = pltpu.SemaphoreType.DMA
    return pl.pallas_call(
        mixer_kernel,
        out_shape=jax.ShapeDtypeStruct((tok_rows, 3 * VAL_DIM), jnp.bfloat16),
        in_specs=[in_hbm] * 3 + [pl.BlockSpec(memory_space=pltpu.SMEM)] + [in_vmem] * 6,
        out_specs=in_vmem,
        scratch_shapes=[
            pltpu.VMEM((Z, Y, FIRST, width), jnp.bfloat16),
            pltpu.VMEM((Z, Y, SECOND, width), jnp.bfloat16),
            pltpu.VMEM((2, tok_rows, 4 * HEAD_DIM), jnp.bfloat16),
            pltpu.VMEM((4, rows, 2 * HEAD_DIM), jnp.bfloat16),
            pltpu.VMEM((4, rows, 128), jnp.float32),
            pltpu.VMEM((4, rows, 128), jnp.float32),
            pltpu.VMEM((4, rows, VAL_DIM), jnp.float32),
            pltpu.VMEM((4, rows, 128), jnp.float32),
            pltpu.VMEM((4, tok_rows, 128), jnp.float32),
            pltpu.VMEM((4, tok_rows, VAL_DIM), jnp.float32),
            pltpu.VMEM((tok_rows, VAL_DIM), jnp.float32),
            pltpu.VMEM((tok_rows, KEY_DIM), jnp.float32),
            pltpu.VMEM((2, KEY_DIM, VAL_DIM), jnp.float32),
            pltpu.VMEM((2, 8, KEY_DIM), jnp.float32),
            pltpu.VMEM((Y, KEY_DIM, VAL_DIM), jnp.bfloat16),
            pltpu.VMEM((Y, 8, KEY_DIM), jnp.float32),
            pltpu.VMEM((2, KEY_DIM, VAL_DIM), jnp.float32),
            dma((5,)),
            dma((Z, Y, 2)),
            dma((Z, Y, 2)),
            dma((Z, 2)),
            dma((Z, 2)),
            dma((Z, 2)),
            dma((2,)),
            dma((2,)),
            dma((Z, Y, 2)),
            dma((5,)),
            dma((5,)),
            dma((3, 2)),
            dma((Y, 2)),
            dma((1,)),
            dma((1,)),
        ],
        compiler_params=pltpu.CompilerParams(
            collective_id=0, has_side_effects=True, vmem_limit_bytes=60 * 1024 * 1024
        ),
        cost_estimate=pl.CostEstimate(
            flops=12 * 10**9, bytes_accessed=16 * 10**6, transcendentals=16 * 10**6
        ),
    )(
        queries,
        keys,
        values,
        lam,
        diff_gain.reshape(1, VAL_DIM),
        lin_query,
        lin_key,
        lin_value,
        decay_pre,
        lin_gain.reshape(1, VAL_DIM),
    )


def body(
    queries,
    keys,
    values,
    lam,
    diff_gain,
    lin_query,
    lin_key,
    lin_value,
    decay_pre,
    lin_gain,
    w_out_diff,
    w_out_lin,
):
    tok_rows = queries.shape[0]
    act = mixer(
        queries, keys, values, lam, diff_gain, lin_query, lin_key, lin_value, decay_pre, lin_gain
    )
    mixed = (
        jnp.dot(act[:, : 2 * VAL_DIM], w_out_diff, preferred_element_type=jnp.float32)
        + jnp.dot(act[:, 2 * VAL_DIM :], w_out_lin, preferred_element_type=jnp.float32)
    ).astype(jnp.bfloat16)
    blocks = mixed.reshape(4, tok_rows // 4, -1)
    arrived = lax.all_to_all(blocks, "tp", split_axis=0, concat_axis=0, tiled=True)
    return arrived.astype(jnp.float32).sum(axis=0).astype(jnp.bfloat16)


def solution(mesh):
    finer = Mesh(mesh.devices.reshape(8, 4, 2, mesh.shape["tp"]), ("sp_0", "sp_1", "sp_2", "tp"))
    in_specs = (
        P(SP, "tp"),
        P(SP, "tp"),
        P(SP, "tp"),
        P("tp"),
        P(),
        P(SP, "tp"),
        P(SP, "tp"),
        P(SP, "tp"),
        P(SP, "tp"),
        P("tp"),
        P("tp", None),
        P("tp", None),
    )
    out_specs = P(SP_TP, None)
    return jax.shard_map(body, mesh=finer, in_specs=in_specs, out_specs=out_specs, check_vma=False)
```

time: 308 us -> 159 us (0.52)
  Pallas kernels: 0 us -> 121 us
  matrix products: 82.9 us -> 5.24 us
  blocking collectives: 92 us -> 30.3 us
  other arithmetic: 43.4 us -> 2.86 us
  waiting for transfers between devices: 35.4 us -> 0 us
  local copies, waits for them, and re-layouts: 26.6 us -> 0.01 us
  between operations: 13.8 us -> 0.03 us
  loops' own time: 11.1 us -> 0 us
    pallas_call x0 -> x1, Pallas kernels: none -> 121 us  [mixer(): pl.pallas_call(mixer_kernel, out_shape=jax.ShapeDtypeStruct((tok_rows, 3...]
    dot_general x47 -> x2, matrix products: 82.9 us -> 5.24 us  [the longest x1 3.53 us: body(): jnp.dot(act[:, :2 * VAL_DIM], w_out_diff, preferred_element_type=jnp.floa...]
    all_gather x6 -> x0, blocking collectives: 62.2 us -> none  [entering(): lax.all_gather(part.astype(kind), axis)]
    all_gather x2 -> x0, waiting for transfers between devices: 34.7 us -> none  [side_by_side(): out = lax.all_gather(both, axis, axis=dim, tiled=True)]
    split x4 -> x0, local copies, waits for them, and re-layouts: 21.5 us -> none  [side_by_side(): jnp.split(out, [sum(widths[:k]) for k in range(1, len(widths))], axis=along)]
    reduce_sum x18 -> x1, other arithmetic: 20.7 us -> 2.86 us  [body(): return arrived.astype(jnp.float32).sum(axis=0).astype(jnp.bfloat16)]
    another operation x19 -> x0, loops' own time: 11.1 us -> none  [the longest x2 9.6 us: attend(): return lax.fori_loop(0, row_count // step_rows, visit, carries)]
    ge x20 -> x0, other arithmetic: 7.42 us -> none  [the longest x16 7.38 us: compute(): allowed = query_pos[:, None] >= key_pos[None, :]]
  transfers between devices with their start and end apart: 2 -> 0, of which waited for: 2 -> 0; matrix products, arithmetic and copies ran while one was open for 26% -> 0% of each run, Pallas kernels for 0% -> 0%
where the time goes in v1:
time: 159 us
  Pallas kernels  121 us (76%)
  blocking collectives  30.3 us (19%)
  matrix products  5.24 us (3%)
  other arithmetic  2.86 us (2%)
    pallas_call x1, Pallas kernels, mixer(): pl.pallas_call(mixer_kernel, out_shape=jax.ShapeDtypeStruct((tok_rows, 3...  121 us
    all_to_all x1, blocking collectives, body(): lax.all_to_all(blocks, 'tp', split_axis=0, concat_axis=0, tiled=True)  30.3 us
    dot_general x1, matrix products, body(): jnp.dot(act[:, :2 * VAL_DIM], w_out_diff, preferred_element_type=jnp.floa...  3.53 us

profile of v1, /device:TPU:225, one launch (start us, length us, event | category | flops | bytes accessed | tf_op | source)
XLA Modules:
  0.0 159.1 jit_solution(2306378324032540016)
XLA Ops:
  0.0 0.0 copy-start
  0.0 120.6 %shard_map.118 = bf16[256,768]{1,0:T(8,128)(2,1)} custom-call(bf16[256,512]{1,0:T(8,128)(2,1)} %q_hbm.1, bf16[256,256]{1,0:T(8,128)(2,1)} %k_hbm.1, bf16[256,256]{1,0:T(8,128)(2,1)} %v_hbm.1, f32[2]{0:T(128)} %lam_ref.1, f32[1,256]{1,0:T(1,128)} %bitcast.6, bf16[256,128]{1,0:T(8,128)(2,1)} %lin_q_ref.1, bf16[256,128]{1,0:T(8,128)(2,1)} %lin_k_ref.1, ...), custom_call_target="tpu_custom_call" | custom-call | flops 12000000000 | bytes 16000000 | tf_op jit(solution)/shard_map/pallas_call | solution.py:596
  120.7 3.5 %fusion.1 = f32[256,4096]{1,0:T(8,128)S(1)} fusion(bf16[512,4096]{1,0:T(8,128)(2,1)} %param.22, bf16[256,768]{1,0:T(8,128)(2,1)} %shard_map.118), kind=kOutput, calls=%fused_computation.2 | convolution fusion | flops 1073741824 | bytes 8650752 | tf_op jit(solution)/shard_map/dot_general | solution.py:674
  124.2 0.0 copy-done
  124.2 1.7 %fusion = bf16[256,4096]{1,0:T(8,128)(2,1)S(1)} fusion(f32[256,4096]{1,0:T(8,128)S(1)} %fusion.1, bf16[256,4096]{1,0:T(8,128)(2,1)S(1)} %copy-done, bf16[256,768]{1,0:T(8,128)(2,1)} %shard_map.118), kind=kOutput, calls=%fused_computation.1 | convolution fusion | flops 538968064 | bytes 8519680 | tf_op jit(solution)/shard_map/dot_general | solution.py:675
  125.9 30.3 %all_to_all.5 = bf16[4,64,4096]{2,1,0:T(8,128)(2,1)} all-to-all(bf16[4,64,4096]{2,1,0:T(8,128)(2,1)S(1)} %bitcast.5), channel_id=1, replica_groups=mesh['sp_0'=8,'sp_1'=4,'sp_2'=2,'tp'=4] {'tp'}, dimensions={0} | all-to-all | bytes 4194304 | tf_op jit(solution)/shard_map/all_to_all | solution.py:678
  156.3 2.9 %reduce_sum.12 = bf16[64,4096]{1,0:T(8,128)(2,1)} reduce(bf16[4,64,4096]{2,1,0:T(8,128)(2,1)} %all_to_all.5, bf16[]{:T(256)} %constant.2.clone.1), dimensions={0}, to_apply=%region_0.0 | reduce | flops 786432 | bytes 2621442 | tf_op jit(solution)/shard_map/reduce_sum | solution.py:679
Async XLA Ops:
  0.0 124.2 %copy-start = (bf16[256,4096]{1,0:T(8,128)(2,1)S(1)}, bf16[256,4096]{1,0:T(8,128)(2,1)}, u32[]{:S(2)}) copy-start(bf16[256,4096]{1,0:T(8,128)(2,1)} %param.23) | copy-start | bytes 6291460

commit v2 on v1

--- a/solution.py
+++ b/solution.py
@@ -75,27 +75,30 @@
     total_ref[...] = jnp.broadcast_to(passed, (8, KEY_DIM))
 
 
-def absorb(q2_ref, keys, values, top_ref, total_ref, numer_ref, group, hidden):
-    scores = dot_nt(q2_ref[group], jnp.concatenate([keys, keys], axis=1))
+def absorb(q2_ref, keys, values, top_ref, total_ref, numer_ref, hidden):
+    scores = dot_nt(q2_ref[...], jnp.concatenate([keys, keys], axis=1))
     if hidden is not None:
         scores = jnp.where(hidden, 2 * neg_large, scores)
-    old_top = top_ref[group][:, :1]
+    old_top = top_ref[:, :1]
     new_top = jnp.maximum(old_top, jnp.max(scores, axis=1, keepdims=True))
     weights = jnp.exp2(scores - new_top)
     shrink = jnp.exp2(old_top - new_top)
     folded = weights[:, :128]
     for tile in range(1, weights.shape[1] // 128):
         folded = folded + weights[:, tile * 128 : (tile + 1) * 128]
-    total_ref[group] = total_ref[group] * shrink + folded
-    top_ref[group] = jnp.broadcast_to(new_top, (new_top.shape[0], 128))
-    numer_ref[group] = numer_ref[group] * shrink + jnp.dot(
+    total_ref[...] = total_ref[...] * shrink + folded
+    top_ref[...] = jnp.broadcast_to(new_top, top_ref.shape)
+    numer_ref[...] = numer_ref[...] * shrink + jnp.dot(
         weights.astype(jnp.bfloat16), values, preferred_element_type=jnp.float32
     )
 
 
+PER_PIECE = 4
+CHUNK = 256
 FIRST = 160
 SECOND = 96
-Z, Y = 8, 4
+Z, Y, TP = 8, 4, 4
+COLUMNS = 1024
 MESH_IDS = pl.DeviceIdType.MESH
 KEY_COLS = slice(0, 2 * HEAD_DIM)
 VALUE_COLS = slice(2 * HEAD_DIM, 2 * HEAD_DIM + VAL_DIM)
@@ -127,7 +130,15 @@
     lin_v_ref,
     decay_ref,
     lin_gain_ref,
+    w_diff_hbm,
+    w_lin_hbm,
+    out_ref,
     act_ref,
+    w_ref,
+    part_ref,
+    far_in,
+    near_out,
+    near_in,
     kva,
     kvb,
     both_q,
@@ -160,6 +171,11 @@
     line_recv,
     chain_send,
     chain_recv,
+    weight_sems,
+    far_send,
+    far_recv,
+    near_send,
+    near_recv,
 ):
     z, y, core = (lax.axis_index(name) for name in SP)
     tok_rows = q_hbm.shape[0]
@@ -168,6 +184,8 @@
     east, west = lax.rem(y + 1, Y), lax.rem(y + Y - 1, Y)
     across = lax.rem(y + 2, Y)
     other = 1 - core
+    x = lax.axis_index("tp")
+    right, left = lax.rem(x + 1, TP), lax.rem(x + TP - 1, TP)
 
     owned = [
         pltpu.make_async_copy(
@@ -194,9 +212,11 @@
         {"sp_1": west},
         {"sp_1": across},
         {"sp_2": other},
+        {"tp": right},
+        {"tp": left},
     ):
         pl.semaphore_signal(barrier, inc=1, device_id=where, device_id_type=MESH_IDS)
-    pl.semaphore_wait(barrier, 6)
+    pl.semaphore_wait(barrier, 8)
     for copy in owned:
         copy.wait()
 
@@ -236,14 +256,21 @@
         both_q.at[core], both_q.at[core], pair_send.at[0], pair_recv.at[0], sp_2=other
     )
     pair_q.start()
-    a_z(z, up, 0).start()
-    a_z(z, down, 1).start()
+    def outward(copy_of):
+        @pl.when(z < Z - 1)
+        def _():
+            copy_of(up, 0).start()
+
+        @pl.when(z < Z // 2)
+        def _():
+            copy_of(down, 1).start()
+
+    outward(lambda toward, way: a_z(z, toward, way))
     b_y(east, 0).start()
     b_y(west, 1).start()
     a_y(z, east, 0).start()
     a_y(z, west, 1).start()
-    b_z(z, y, up, 0).start()
-    b_z(z, y, down, 1).start()
+    outward(lambda toward, way: b_z(z, y, toward, way))
 
     linear_kernel(
         lin_q_ref,
@@ -266,12 +293,19 @@
 
     b_wait(z, west)
     b_far(west, east, 0).start()
-    b_z(z, west, up, 0).start()
-    b_z(z, west, down, 1).start()
+    outward(lambda toward, way: b_z(z, west, toward, way))
     b_wait(z, east)
     b_far(east, west, 1).start()
-    b_z(z, east, up, 0).start()
-    b_z(z, east, down, 1).start()
+    outward(lambda toward, way: b_z(z, east, toward, way))
+
+    weights = (
+        pltpu.make_async_copy(w_diff_hbm, w_ref.at[pl.ds(0, 2 * VAL_DIM)], weight_sems.at[0]),
+        pltpu.make_async_copy(
+            w_lin_hbm, w_ref.at[pl.ds(2 * VAL_DIM, VAL_DIM)], weight_sems.at[1]
+        ),
+    )
+    for copy in weights:
+        copy.start()
 
     top_ref[...] = jnp.full_like(top_ref, neg_large)
     total_ref[...] = jnp.zeros_like(total_ref)
@@ -297,8 +331,7 @@
 
     b_wait(z, across, KEY_COLS, 0)
     b_wait(z, across, VALUE_COLS, 1)
-    b_z(z, across, up, 0).start()
-    b_z(z, across, down, 1).start()
+    outward(lambda toward, way: b_z(z, across, toward, way))
 
     def line(peer, index):
         return (
@@ -348,53 +381,102 @@
         z + 2 * Z + jnp.where(lax.rem(unit, 2) == 1, -((unit + 1) // 2), unit // 2), Z
     )
 
-    def compute(store, zo, group, hidden):
-        mapping = group // 2
-        tokens = store.shape[2]
-        first = pl.multiple_of(mapping * HEAD_DIM, HEAD_DIM)
-        keys = store[zo, :, :, pl.ds(first, HEAD_DIM)].reshape(Y * tokens, HEAD_DIM)
-        values = store[zo, :, :, VALUE_COLS].reshape(Y * tokens, VAL_DIM)
-        absorb(q2_ref, keys, values, top_ref, total_ref, numer_ref, group, hidden)
-
-    def hidden_from(tokens, start):
-        column = lax.broadcasted_iota(jnp.int32, (chip_rows, Y * tokens), 1)
-        row = lax.broadcasted_iota(jnp.int32, (chip_rows, Y * tokens), 0)
-        chip = jnp.zeros_like(column)
+    def compute(zo, index, hidden):
+        values = jnp.concatenate(
+            [
+                store[zo, :, :, VALUE_COLS].reshape(Y * store.shape[2], VAL_DIM)
+                for store in (kva, kvb)
+            ],
+            axis=0,
+        )
+        for step in range(PER_PIECE):
+            group = index * PER_PIECE + step
+            first = pl.multiple_of(group // 2 * HEAD_DIM, HEAD_DIM)
+            keys = jnp.concatenate(
+                [
+                    store[zo, :, :, pl.ds(first, HEAD_DIM)].reshape(
+                        Y * store.shape[2], HEAD_DIM
+                    )
+                    for store in (kva, kvb)
+                ],
+                axis=0,
+            )
+            for part in range(0, chip_rows, CHUNK):
+                rows = slice(part, part + CHUNK)
+                absorb(
+                    q2_ref.at[group, rows],
+                    keys,
+                    values,
+                    top_ref.at[group, rows],
+                    total_ref.at[group, rows],
+                    numer_ref.at[group, rows],
+                    None if hidden is None else hidden[rows],
+                )
+
+    def hidden_keys():
+        column = lax.broadcasted_iota(jnp.int32, (chip_rows, Y * tok_rows), 1)
+        row = lax.broadcasted_iota(jnp.int32, (chip_rows, Y * tok_rows), 0)
+        key_pos = column + core * tok_rows
         for index in range(1, Y):
-            chip = chip + jnp.where(column >= index * tokens, 1, 0)
-        key_pos = column + chip * (chip_rows - tokens) + core * tok_rows + start
+            key_pos = key_pos + jnp.where(column >= index * FIRST, chip_rows - FIRST, 0)
+        key_pos = key_pos + jnp.where(
+            column >= Y * FIRST, FIRST - Y * FIRST - (Y - 1) * (chip_rows - FIRST), 0
+        )
+        for index in range(1, Y):
+            key_pos = key_pos + jnp.where(
+                column >= Y * FIRST + index * SECOND, chip_rows - SECOND, 0
+            )
         return key_pos > y * chip_rows + row
 
     def a_step(distance):
-        for way, zo, toward in (
-            (0, lax.rem(z + Z - distance, Z), up),
-            (1, lax.rem(z + distance, Z), down),
-        ):
-            a_wait(zo, y)
+        ahead, behind = lax.rem(z + Z - distance, Z), lax.rem(z + distance, Z)
+
+        @pl.when(z >= distance)
+        def _():
+            a_wait(ahead, y)
+
+            @pl.when((distance < 3) & (z < Z - 1))
+            def _():
+                a_z(ahead, up, 0).start()
+
+            @pl.when((distance == 3) & (z < Z - 1))
+            def _():
+                a_z(ahead, up, 0, KEY_COLS, 0).start()
+
+            a_y(ahead, east, 0).start()
+            a_y(ahead, west, 1).start()
+
+        @pl.when(behind < Z // 2)
+        def _():
+            a_wait(behind, y)
 
             @pl.when(distance < 3)
             def _():
-                a_z(zo, toward, way).start()
+                a_z(behind, down, 1).start()
 
             @pl.when(distance == 3)
             def _():
-                a_z(zo, toward, way, (KEY_COLS, VALUE_COLS)[way], way).start()
-
-            a_y(zo, east, 0).start()
-            a_y(zo, west, 1).start()
+                a_z(behind, down, 1, VALUE_COLS, 1).start()
+
+            @pl.when(behind < z)
+            def _():
+                a_y(behind, east, 0).start()
+                a_y(behind, west, 1).start()
 
     def a_near(zo):
-        a_wait(zo, west)
-        a_far(zo, west, east, 0).start()
-        a_wait(zo, east)
-        a_far(zo, east, west, 1).start()
+        @pl.when(zo <= z)
+        def _():
+            a_wait(zo, west)
+            a_far(zo, west, east, 0).start()
+            a_wait(zo, east)
+            a_far(zo, east, west, 1).start()
 
     def half_step(h, carry):
         @pl.when(h <= 2)
         def _():
             a_step(h + 1)
 
-        @pl.when(h == 3)
+        @pl.when((h == 3) & (z >= Z // 2))
         def _():
             zo = lax.rem(z + 4, Z)
             a_wait(zo, y, KEY_COLS, 0)
@@ -415,32 +497,32 @@
         def _():
             a_near(lax.rem(z + 4, Z))
 
-        a_unit, b_unit = h - 2, h - 1
-        a_origin, b_origin = origin(jnp.maximum(a_unit, 0)), origin(jnp.maximum(b_unit, 0))
-
-        @pl.when(h >= 2)
-        def _():
-            a_wait(a_origin, across, KEY_COLS, 0)
-            a_wait(a_origin, across, VALUE_COLS, 1)
-
-        def piece(j, inner):
+        unit = h - 2
+        zo_unit = origin(jnp.maximum(unit, 0))
+
+        @pl.when((unit == 0) | ((unit > 0) & (zo_unit < z)))
+        def _():
+            a_wait(zo_unit, across, KEY_COLS, 0)
+            a_wait(zo_unit, across, VALUE_COLS, 1)
+
+        def event(j):
             distance = h // 2 + 1
             yo = order(lax.rem(h, 2) * 2 + j // 2)
             ahead, behind = lax.rem(z + Z - distance, Z), lax.rem(z + distance, Z)
 
-            @pl.when((h <= 5) & (lax.rem(j, 2) == 0))
+            @pl.when((h <= 5) & (lax.rem(j, 2) == 0) & (z >= distance))
             def _():
                 b_wait(ahead, yo)
 
-                @pl.when(distance < 3)
+                @pl.when((distance < 3) & (z < Z - 1))
                 def _():
                     b_z(ahead, yo, up, 0).start()
 
-                @pl.when(distance == 3)
+                @pl.when((distance == 3) & (z < Z - 1))
                 def _():
                     b_z(ahead, yo, up, 0, KEY_COLS, 0).start()
 
-            @pl.when((h <= 5) & (lax.rem(j, 2) == 1))
+            @pl.when((h <= 5) & (lax.rem(j, 2) == 1) & (behind < Z // 2))
             def _():
                 b_wait(behind, yo)
 
@@ -452,7 +534,7 @@
                 def _():
                     b_z(behind, yo, down, 1, VALUE_COLS, 1).start()
 
-            @pl.when(((h == 6) | (h == 7)) & (lax.rem(j, 2) == 1))
+            @pl.when(((h == 6) | (h == 7)) & (lax.rem(j, 2) == 1) & (z >= Z // 2))
             def _():
                 b_wait(ahead, yo, KEY_COLS, 0)
                 b_wait(ahead, yo, VALUE_COLS, 1)
@@ -469,21 +551,17 @@
                 def _():
                     pass_on()
 
-            @pl.when((h >= 2) & (a_unit > 0) & (a_origin < z))
-            def _():
-                compute(kva, a_origin, j, None)
-
-            @pl.when(a_unit == 0)
-            def _():
-                compute(kva, z, j, hidden_from(FIRST, 0))
-
-            @pl.when((b_unit > 0) & (h <= 8) & (b_origin < z))
-            def _():
-                compute(kvb, b_origin, j, None)
-
-            @pl.when(b_unit == 0)
-            def _():
-                compute(kvb, z, j, hidden_from(SECOND, FIRST))
+        def piece(j, inner):
+            for step in range(PER_PIECE):
+                event(j * PER_PIECE + step)
+
+            @pl.when((unit > 0) & (zo_unit < z))
+            def _():
+                compute(zo_unit, j, None)
+
+            @pl.when(unit == 0)
+            def _():
+                compute(z, j, hidden_keys())
 
             return inner
 
@@ -499,7 +577,7 @@
                         sp_1=peer,
                     ).wait_recv()
 
-        return lax.fori_loop(0, 4, piece, carry)
+        return lax.fori_loop(0, 4 // PER_PIECE, piece, carry)
 
     lax.fori_loop(0, 10, half_step, 0)
 
@@ -546,6 +624,76 @@
             attended, diff_gain_ref[...]
         ).astype(act_ref.dtype)
 
+    own_rows = tok_rows // TP
+    half = COLUMNS // 2
+    halves = (slice(0, half), slice(half, COLUMNS))
+    rows_of = lambda member: pl.ds(pl.multiple_of(member * own_rows, own_rows), own_rows)
+    toward = (right, left)
+    opposite = lax.rem(x + 2, TP)
+    for copy in weights:
+        copy.wait()
+
+    def far_copy(chunk, way):
+        return remote(
+            part_ref.at[chunk, rows_of(opposite), halves[way]],
+            far_in.at[chunk, way],
+            far_send.at[chunk, way],
+            far_recv.at[chunk, way],
+            tp=toward[way],
+        )
+
+    def near_copy(chunk, way):
+        return remote(
+            near_out.at[chunk, way],
+            near_in.at[chunk, way],
+            near_send.at[chunk, way],
+            near_recv.at[chunk, way],
+            tp=toward[way],
+        )
+
+    chunks = part_ref.shape[0]
+
+    def project(chunk, carry):
+        first = pl.multiple_of(chunk * COLUMNS, COLUMNS)
+        part_ref[chunk] = jnp.dot(
+            act_ref[...], w_ref[:, pl.ds(first, COLUMNS)], preferred_element_type=jnp.float32
+        ).astype(part_ref.dtype)
+        for way in range(2):
+            far_copy(chunk, way).start()
+        return carry
+
+    lax.fori_loop(0, chunks, project, 0)
+
+    def meet(chunk, carry):
+        for way in range(2):
+            far_copy(chunk, way).wait_recv()
+            near = part_ref[chunk, rows_of(toward[way])].astype(jnp.float32)
+            here = near[:, halves[way]] + far_in[chunk, way].astype(jnp.float32)
+            sides = (here, near[:, halves[1]]) if way == 0 else (near[:, halves[0]], here)
+            near_out[chunk, way] = jnp.concatenate(sides, axis=1).astype(near_out.dtype)
+            near_copy(chunk, way).start()
+        return carry
+
+    lax.fori_loop(0, chunks, meet, 0)
+
+    def finish(chunk, carry):
+        total = part_ref[chunk, rows_of(x)].astype(jnp.float32)
+        for way in range(2):
+            near_copy(chunk, way).wait_recv()
+            total = total + near_in[chunk, way].astype(jnp.float32)
+        first = pl.multiple_of(chunk * COLUMNS, COLUMNS)
+        out_ref[:, pl.ds(first, COLUMNS)] = total.astype(out_ref.dtype)
+        return carry
+
+    lax.fori_loop(0, chunks, finish, 0)
+
+    def drain_out(chunk, carry):
+        for way in range(2):
+            far_copy(chunk, way).wait_send()
+            near_copy(chunk, way).wait_send()
+        return carry
+
+    lax.fori_loop(0, chunks, drain_out, 0)
     for copy in (pair_q, pair_state, pair_decay, swap_numer, swap_stat):
         copy.wait_send()
     for index, peer in enumerate((east, west, across)):
@@ -561,33 +709,59 @@
         b_far(west if way == 0 else east, toward, way).wait_send()
 
     def drain(offset, carry):
-        zo = lax.rem(z + offset, Z)
+        zo = z - offset
         for way, toward in ((0, east), (1, west)):
             a_y(zo, toward, way).wait_send()
             a_far(zo, west if way == 0 else east, toward, way).wait_send()
         return carry
 
-    lax.fori_loop(0, Z, drain, 0)
-    for way, toward, sign, cols in ((0, up, -1, KEY_COLS), (1, down, 1, VALUE_COLS)):
-
-        def drain_z(distance, carry):
-            zo = lax.rem(z + Z + sign * distance, Z)
-            a_z(zo, toward, way).wait_send()
+    lax.fori_loop(0, z + 1, drain, 0)
+
+    @pl.when(z < Z - 1)
+    def _():
+        def drain_up(offset, carry):
+            a_z(z - offset, up, 0).wait_send()
             for yo in range(Y):
-                b_z(zo, yo, toward, way).wait_send()
+                b_z(z - offset, yo, up, 0).wait_send()
             return carry
 
-        lax.fori_loop(0, 3, drain_z, 0)
-        zo = lax.rem(z + Z + sign * 3, Z)
-        a_z(zo, toward, way, cols, way).wait_send()
-        for yo in range(Y):
-            b_z(zo, yo, toward, way, cols, way).wait_send()
-
-
-def mixer(
-    queries, keys, values, lam, diff_gain, lin_query, lin_key, lin_value, decay_pre, lin_gain
+        lax.fori_loop(0, jnp.minimum(z + 1, 3), drain_up, 0)
+
+        @pl.when(z >= 3)
+        def _():
+            a_z(z - 3, up, 0, KEY_COLS, 0).wait_send()
+            for yo in range(Y):
+                b_z(z - 3, yo, up, 0, KEY_COLS, 0).wait_send()
+
+    for distance in range(4):
+        zo = lax.rem(z + distance, Z)
+        part = (VALUE_COLS, 1) if distance == 3 else ()
+
+        @pl.when(zo < Z // 2)
+        def _(zo=zo, part=part):
+            a_z(zo, down, 1, *part).wait_send()
+            for yo in range(Y):
+                b_z(zo, yo, down, 1, *part).wait_send()
+
+
+def body(
+    queries,
+    keys,
+    values,
+    lam,
+    diff_gain,
+    lin_query,
+    lin_key,
+    lin_value,
+    decay_pre,
+    lin_gain,
+    w_out_diff,
+    w_out_lin,
 ):
     tok_rows = queries.shape[0]
+    depth = w_out_diff.shape[0] + w_out_lin.shape[0]
+    model = w_out_diff.shape[1]
+    chunks, own_rows = model // COLUMNS, tok_rows // TP
     rows = 2 * tok_rows
     width = 2 * HEAD_DIM + VAL_DIM
     in_hbm = pl.BlockSpec(memory_space=pl.ANY)
@@ -595,10 +769,19 @@
     dma = pltpu.SemaphoreType.DMA
     return pl.pallas_call(
         mixer_kernel,
-        out_shape=jax.ShapeDtypeStruct((tok_rows, 3 * VAL_DIM), jnp.bfloat16),
-        in_specs=[in_hbm] * 3 + [pl.BlockSpec(memory_space=pltpu.SMEM)] + [in_vmem] * 6,
+        out_shape=jax.ShapeDtypeStruct((own_rows, model), jnp.bfloat16),
+        in_specs=[in_hbm] * 3
+        + [pl.BlockSpec(memory_space=pltpu.SMEM)]
+        + [in_vmem] * 6
+        + [in_hbm] * 2,
         out_specs=in_vmem,
         scratch_shapes=[
+            pltpu.VMEM((tok_rows, 3 * VAL_DIM), jnp.bfloat16),
+            pltpu.VMEM((depth, model), jnp.bfloat16),
+            pltpu.VMEM((chunks, tok_rows, COLUMNS), jnp.bfloat16),
+            pltpu.VMEM((chunks, 2, own_rows, COLUMNS // 2), jnp.bfloat16),
+            pltpu.VMEM((chunks, 2, own_rows, COLUMNS), jnp.bfloat16),
+            pltpu.VMEM((chunks, 2, own_rows, COLUMNS), jnp.bfloat16),
             pltpu.VMEM((Z, Y, FIRST, width), jnp.bfloat16),
             pltpu.VMEM((Z, Y, SECOND, width), jnp.bfloat16),
             pltpu.VMEM((2, tok_rows, 4 * HEAD_DIM), jnp.bfloat16),
@@ -631,6 +814,11 @@
             dma((Y, 2)),
             dma((1,)),
             dma((1,)),
+            dma((2,)),
+            dma((chunks, 2)),
+            dma((chunks, 2)),
+            dma((chunks, 2)),
+            dma((chunks, 2)),
         ],
         compiler_params=pltpu.CompilerParams(
             collective_id=0, has_side_effects=True, vmem_limit_bytes=60 * 1024 * 1024
@@ -649,34 +837,9 @@
         lin_value,
         decay_pre,
         lin_gain.reshape(1, VAL_DIM),
-    )
-
-
-def body(
-    queries,
-    keys,
-    values,
-    lam,
-    diff_gain,
-    lin_query,
-    lin_key,
-    lin_value,
-    decay_pre,
-    lin_gain,
-    w_out_diff,
-    w_out_lin,
-):
-    tok_rows = queries.shape[0]
-    act = mixer(
-        queries, keys, values, lam, diff_gain, lin_query, lin_key, lin_value, decay_pre, lin_gain
-    )
-    mixed = (
-        jnp.dot(act[:, : 2 * VAL_DIM], w_out_diff, preferred_element_type=jnp.float32)
-        + jnp.dot(act[:, 2 * VAL_DIM :], w_out_lin, preferred_element_type=jnp.float32)
-    ).astype(jnp.bfloat16)
-    blocks = mixed.reshape(4, tok_rows // 4, -1)
-    arrived = lax.all_to_all(blocks, "tp", split_axis=0, concat_axis=0, tiled=True)
-    return arrived.astype(jnp.float32).sum(axis=0).astype(jnp.bfloat16)
+        w_out_diff,
+        w_out_lin,
+    )
 
 
 def solution(mesh):

time: 159 us -> 109 us (0.69)
  blocking collectives: 30.3 us -> 0 us
  Pallas kernels: 121 us -> 107 us
  matrix products: 5.24 us -> 0 us
  other arithmetic: 2.86 us -> 0 us
  local copies, waits for them, and re-layouts: 0.01 us -> 1.87 us
    all_to_all x1 -> x0, blocking collectives: 30.3 us -> none  [body(): lax.all_to_all(blocks, 'tp', split_axis=0, concat_axis=0, tiled=True)]
    pallas_call x1, Pallas kernels: 121 us -> 107 us  [body(): pl.pallas_call(mixer_kernel, out_shape=jax.ShapeDtypeStruct((own_rows, mo...]
    dot_general x2 -> x0, matrix products: 5.24 us -> none  [the longest x1 3.53 us: body(): jnp.dot(act[:, :2 * VAL_DIM], w_out_diff, preferred_element_type=jnp.floa...]
    reduce_sum x1 -> x0, other arithmetic: 2.86 us -> none  [body(): return arrived.astype(jnp.float32).sum(axis=0).astype(jnp.bfloat16)]
    unnamed x2 -> x1, local copies, waits for them, and re-layouts: 0.01 us -> 1.87 us
where the time goes in v2:
time: 109 us
  Pallas kernels  107 us (98%)
  local copies, waits for them, and re-layouts  1.87 us (2%)
    pallas_call x1, Pallas kernels, body(): pl.pallas_call(mixer_kernel, out_shape=jax.ShapeDtypeStruct((own_rows, mo...  107 us

profile of v2, /device:TPU:225, one launch (start us, length us, event | category | flops | bytes accessed | tf_op | source)
XLA Modules:
  0.0 108.5 jit_solution(16898416704988988930)
XLA Ops:
  0.0 106.7 %shard_map.118 = bf16[64,4096]{1,0:T(8,128)(2,1)} custom-call(bf16[256,512]{1,0:T(8,128)(2,1)} %q_hbm.1, bf16[256,256]{1,0:T(8,128)(2,1)} %k_hbm.1, bf16[256,256]{1,0:T(8,128)(2,1)} %v_hbm.1, f32[2]{0:T(128)} %lam_ref.1, f32[1,256]{1,0:T(1,128)} %bitcast.2, bf16[256,128]{1,0:T(8,128)(2,1)} %lin_q_ref.1, bf16[256,128]{1,0:T(8,128)(2,1)} %lin_k_ref.1, ...), custom_call_target="tpu_custom_call" | custom-call | flops 12000000000 | bytes 16000000 | tf_op jit(solution)/shard_map/pallas_call | solution.py:770
  106.7 1.9 %copy.14 = bf16[64,4096]{1,0:T(8,128)(2,1)} copy(bf16[64,4096]{1,0:T(8,128)(2,1)} %shard_map.118) | data formatting | bytes 1048576

commit v3 on v2

--- a/solution.py
+++ b/solution.py
@@ -291,6 +291,43 @@
     pair_state.start()
     pair_decay.start()
 
+    def a_step(distance):
+        ahead, behind = lax.rem(z + Z - distance, Z), lax.rem(z + distance, Z)
+
+        @pl.when(z >= distance)
+        def _():
+            a_wait(ahead, y)
+
+            @pl.when((distance < 3) & (z < Z - 1))
+            def _():
+                a_z(ahead, up, 0).start()
+
+            @pl.when((distance == 3) & (z < Z - 1))
+            def _():
+                a_z(ahead, up, 0, KEY_COLS, 0).start()
+
+            a_y(ahead, east, 0).start()
+            a_y(ahead, west, 1).start()
+
+        @pl.when(behind < Z // 2)
+        def _():
+            a_wait(behind, y)
+
+            @pl.when(distance < 3)
+            def _():
+                a_z(behind, down, 1).start()
+
+            @pl.when(distance == 3)
+            def _():
+                a_z(behind, down, 1, VALUE_COLS, 1).start()
+
+            @pl.when(behind < z)
+            def _():
+                a_y(behind, east, 0).start()
+                a_y(behind, west, 1).start()
+
+    a_step(jnp.int32(1))
+
     b_wait(z, west)
     b_far(west, east, 0).start()
     outward(lambda toward, way: b_z(z, west, toward, way))
@@ -428,41 +465,6 @@
             )
         return key_pos > y * chip_rows + row
 
-    def a_step(distance):
-        ahead, behind = lax.rem(z + Z - distance, Z), lax.rem(z + distance, Z)
-
-        @pl.when(z >= distance)
-        def _():
-            a_wait(ahead, y)
-
-            @pl.when((distance < 3) & (z < Z - 1))
-            def _():
-                a_z(ahead, up, 0).start()
-
-            @pl.when((distance == 3) & (z < Z - 1))
-            def _():
-                a_z(ahead, up, 0, KEY_COLS, 0).start()
-
-            a_y(ahead, east, 0).start()
-            a_y(ahead, west, 1).start()
-
-        @pl.when(behind < Z // 2)
-        def _():
-            a_wait(behind, y)
-
-            @pl.when(distance < 3)
-            def _():
-                a_z(behind, down, 1).start()
-
-            @pl.when(distance == 3)
-            def _():
-                a_z(behind, down, 1, VALUE_COLS, 1).start()
-
-            @pl.when(behind < z)
-            def _():
-                a_y(behind, east, 0).start()
-                a_y(behind, west, 1).start()
-
     def a_near(zo):
         @pl.when(zo <= z)
         def _():
@@ -472,9 +474,9 @@
             a_far(zo, east, west, 1).start()
 
     def half_step(h, carry):
-        @pl.when(h <= 2)
-        def _():
-            a_step(h + 1)
+        @pl.when((h == 0) | (h == 2))
+        def _():
+            a_step(2 + h // 2)
 
         @pl.when((h == 3) & (z >= Z // 2))
         def _():
@@ -488,29 +490,48 @@
         def _():
             a_near(z)
 
-        @pl.when((h == 2) | (h == 4) | (h == 6))
-        def _():
-            a_near(lax.rem(z + Z - h // 2, Z))
-            a_near(lax.rem(z + h // 2, Z))
-
-        @pl.when(h == 8)
+        @pl.when((h == 3) | (h == 5))
+        def _():
+            a_near(lax.rem(z + Z - (h + 1) // 2, Z))
+            a_near(lax.rem(z + (h + 1) // 2, Z))
+
+        @pl.when(h == 6)
         def _():
             a_near(lax.rem(z + 4, Z))
 
-        unit = h - 2
+        unit = h - 1
         zo_unit = origin(jnp.maximum(unit, 0))
+
+        @pl.when((h == 8) & (z >= Z // 2))
+        def _():
+            for yo in (y, west, east, across):
+                b_wait(lax.rem(z + 4, Z), yo, KEY_COLS, 0)
+                b_wait(lax.rem(z + 4, Z), yo, VALUE_COLS, 1)
 
         @pl.when((unit == 0) | ((unit > 0) & (zo_unit < z)))
         def _():
             a_wait(zo_unit, across, KEY_COLS, 0)
             a_wait(zo_unit, across, VALUE_COLS, 1)
+
+        @pl.when((unit > 0) & (zo_unit < z))
+        def _():
+            compute(zo_unit, 0, None)
+
+        @pl.when(unit == 0)
+        def _():
+            compute(z, 0, hidden_keys())
+
+        @pl.when(h == 1)
+        def _():
+            a_near(lax.rem(z + Z - 1, Z))
+            a_near(lax.rem(z + 1, Z))
 
         def event(j):
             distance = h // 2 + 1
             yo = order(lax.rem(h, 2) * 2 + j // 2)
             ahead, behind = lax.rem(z + Z - distance, Z), lax.rem(z + distance, Z)
 
-            @pl.when((h <= 5) & (lax.rem(j, 2) == 0) & (z >= distance))
+            @pl.when((h <= 5) & (j % 2 == 0) & (z >= distance))
             def _():
                 b_wait(ahead, yo)
 
@@ -522,7 +543,7 @@
                 def _():
                     b_z(ahead, yo, up, 0, KEY_COLS, 0).start()
 
-            @pl.when((h <= 5) & (lax.rem(j, 2) == 1) & (behind < Z // 2))
+            @pl.when((h <= 5) & (j % 2 == 1) & (behind < Z // 2))
             def _():
                 b_wait(behind, yo)
 
@@ -534,14 +555,9 @@
                 def _():
                     b_z(behind, yo, down, 1, VALUE_COLS, 1).start()
 
-            @pl.when(((h == 6) | (h == 7)) & (lax.rem(j, 2) == 1) & (z >= Z // 2))
-            def _():
-                b_wait(ahead, yo, KEY_COLS, 0)
-                b_wait(ahead, yo, VALUE_COLS, 1)
-
             slot = (h - 1) * 2 + j // 2
 
-            @pl.when((h >= 1) & (lax.rem(j, 2) == 0) & (slot == z))
+            @pl.when((h >= 1) & (j % 2 == 0) & (slot == z))
             def _():
                 @pl.when(z > 0)
                 def _():
@@ -550,20 +566,6 @@
                 @pl.when(z < Z - 1)
                 def _():
                     pass_on()
-
-        def piece(j, inner):
-            for step in range(PER_PIECE):
-                event(j * PER_PIECE + step)
-
-            @pl.when((unit > 0) & (zo_unit < z))
-            def _():
-                compute(zo_unit, j, None)
-
-            @pl.when(unit == 0)
-            def _():
-                compute(z, j, hidden_keys())
-
-            return inner
 
         @pl.when(h == 1)
         def _():
@@ -577,9 +579,11 @@
                         sp_1=peer,
                     ).wait_recv()
 
-        return lax.fori_loop(0, 4 // PER_PIECE, piece, carry)
-
-    lax.fori_loop(0, 10, half_step, 0)
+        for j in range(4):
+            event(j)
+        return carry
+
+    lax.fori_loop(0, 9, half_step, 0)
 
     lane = lax.broadcasted_iota(jnp.int32, (chip_rows, 128), 1)
     for group in range(4):

time: 109 us -> 106 us (0.972)
  Pallas kernels: 107 us -> 104 us
    pallas_call x1, Pallas kernels: 107 us -> 104 us  [body(): pl.pallas_call(mixer_kernel, out_shape=jax.ShapeDtypeStruct((own_rows, mo...]
where the time goes in v3:
time: 106 us
  Pallas kernels  104 us (98%)
  local copies, waits for them, and re-layouts  1.87 us (2%)
    pallas_call x1, Pallas kernels, body(): pl.pallas_call(mixer_kernel, out_shape=jax.ShapeDtypeStruct((own_rows, mo...  104 us

profile of v3, /device:TPU:225, one launch (start us, length us, event | category | flops | bytes accessed | tf_op | source)
XLA Modules:
  0.0 105.7 jit_solution(4379249912479876470)
XLA Ops:
  0.0 103.8 %shard_map.118 = bf16[64,4096]{1,0:T(8,128)(2,1)} custom-call(bf16[256,512]{1,0:T(8,128)(2,1)} %q_hbm.1, bf16[256,256]{1,0:T(8,128)(2,1)} %k_hbm.1, bf16[256,256]{1,0:T(8,128)(2,1)} %v_hbm.1, f32[2]{0:T(128)} %lam_ref.1, f32[1,256]{1,0:T(1,128)} %bitcast.2, bf16[256,128]{1,0:T(8,128)(2,1)} %lin_q_ref.1, bf16[256,128]{1,0:T(8,128)(2,1)} %lin_k_ref.1, ...), custom_call_target="tpu_custom_call" | custom-call | flops 12000000000 | bytes 16000000 | tf_op jit(solution)/shard_map/pallas_call | solution.py:774
  103.8 1.9 %copy.14 = bf16[64,4096]{1,0:T(8,128)(2,1)} copy(bf16[64,4096]{1,0:T(8,128)(2,1)} %shard_map.118) | data formatting | bytes 1048576
